TPU v7x, 32 devices: a whole 2x2x4 slice. The times are simulated.
32 devices in a mesh: fs: 16 (over z, y, x), tp: 2 (over core).
Axes of the slice: x: 2, y: 2, z: 4, core: 2. Of those that a mesh axis runs over, the one named last changes fastest.
Arguments:
- tokens: bfloat16 [8192, 2048], P('fs', 'tp'), may hold values from -6 to 6
- norm_gain: bfloat16 [2048], P('tp'), may hold values from 0.099609375 to 1.8984375
- proj_u: bfloat16 [2048, 2048], P('fs', 'tp'), may hold values from -0.125 to 0.125
- proj_v: bfloat16 [2048, 2048], P('fs', 'tp'), may hold values from -0.125 to 0.125
- layer_gain: bfloat16 [2048], P('tp'), may hold values from 0.099609375 to 1.8984375
- layer_shift: bfloat16 [2048], P('tp'), may hold values from -3 to 3
- mix_weight: bfloat16 [16, 128, 128], P('tp'), may hold values from -0.5 to 0.5
- mix_bias: bfloat16 [16, 128], P('tp'), may hold values from 0.099609375 to 1.8984375
- proj_out: bfloat16 [2048, 2048], P('tp', 'fs'), may hold values from -0.1875 to 0.1875
- ffn_gain: bfloat16 [2048], P('tp'), may hold values from 0.099609375 to 1.8984375
- ffn_gate: bfloat16 [2048, 4096], P('fs', 'tp'), may hold values from -0.125 to 0.125
- ffn_value: bfloat16 [2048, 4096], P('fs', 'tp'), may hold values from -0.125 to 0.125
- conv_gate: bfloat16 [3, 4096], P(None, 'tp'), may hold values from -3 to 3
- conv_value: bfloat16 [3, 4096], P(None, 'tp'), may hold values from -3 to 3
- proj_down: bfloat16 [4096, 2048], P('tp', 'fs'), may hold values from -0.125 to 0.125
Outputs:
- result: bfloat16 [8192, 2048], P('fs', 'tp')
All inputs are finite; a program needn't handle non-finite values.
Results may differ from a plain program's by a relative error of at most 0.017.
Values may be sent and summed in bfloat16 or wider, within the bound.
A program may use at most 64 MiB of HBM per device.

v0:
```python
import functools

import jax
import jax.numpy as jnp
from jax import lax
from jax.experimental import pallas as pl
from jax.experimental.pallas import tpu as pltpu
from jax.sharding import PartitionSpec as P

MESH = pl.DeviceIdType.MESH
LANES = 128

GROUP_DIM = 128
BLOCK = 128
SEGMENT = 64
KERNEL = 3
SEQ_LEN = 256


EPS = 1e-06


def matmul(operand, matrix):
    return jnp.dot(operand, matrix, preferred_element_type=jnp.float32)


def local_rms(values_in, gain_row):
    values = values_in.astype(jnp.float32)
    scale_row = lax.rsqrt(jnp.mean(values * values, axis=1, keepdims=True) + EPS)
    return (values * scale_row * gain_row.astype(jnp.float32)).astype(jnp.bfloat16)


def causal_taps(values, weights):
    seq_count = values.shape[0] // SEQ_LEN
    shaped = values.reshape(seq_count, SEQ_LEN, values.shape[1])
    padded = jnp.pad(shaped, ((0, 0), (KERNEL - 1, 0), (0, 0)))
    summed = jnp.zeros(shaped.shape, jnp.float32)
    for tap_index in range(KERNEL):
        summed = summed + padded[:, tap_index : tap_index + SEQ_LEN].astype(jnp.float32) * weights[
            tap_index
        ].astype(jnp.float32)
    return summed.reshape(values.shape[0], values.shape[1])


def on_device(
    tokens,
    norm_gain,
    proj_u,
    proj_v,
    layer_gain,
    layer_shift,
    mix_weight,
    mix_bias,
    proj_out,
    ffn_gain,
    ffn_gate,
    ffn_value,
    conv_gate,
    conv_value,
    proj_down,
):
    own_width = tokens.shape[1]
    whole_tokens, whole_gain, whole_ffn_gain = (
        lax.all_gather(tokens, "tp", axis=1, tiled=True),
        lax.all_gather(norm_gain, "tp", axis=0, tiled=True),
        lax.all_gather(ffn_gain, "tp", axis=0, tiled=True),
    )
    normed = local_rms(whole_tokens, whole_gain)
    row_count = normed.shape[0]
    whole_u, whole_v = (
        lax.all_gather(proj_u, "fs", axis=0, tiled=True),
        lax.all_gather(proj_v, "fs", axis=0, tiled=True),
    )
    pre_u = matmul(normed, whole_u)
    pre_v = matmul(normed, whole_v)
    act_u = jax.nn.gelu(pre_u, approximate=False)
    act_v = jax.nn.gelu(pre_v, approximate=False)
    full_width = act_v.shape[1] * lax.axis_size("tp")
    total_sum, second = lax.psum((jnp.sum(act_v, axis=1), jnp.sum(act_v * act_v, axis=1)), "tp")
    center = total_sum / full_width
    spread = second / full_width - center * center
    mixed_in = (
        (act_v - center[:, None])
        * lax.rsqrt(spread + EPS)[:, None]
        * layer_gain.astype(jnp.float32)
        + layer_shift.astype(jnp.float32)
    ).astype(jnp.bfloat16)
    groups = mixed_in.shape[1] // GROUP_DIM
    blocks = mixed_in.reshape(row_count // BLOCK, BLOCK, groups, GROUP_DIM)
    segment = jnp.arange(BLOCK) // SEGMENT
    visible = segment[None, :] <= segment[:, None]
    masked = jnp.where(visible[None], mix_weight, jnp.zeros_like(mix_weight))
    spatial = (
        jnp.einsum("gij,njgc->nigc", masked, blocks, preferred_element_type=jnp.float32)
        + mix_bias.astype(jnp.float32).T[None, :, :, None]
    )
    gated_rows = (act_u * spatial.reshape(row_count, mixed_in.shape[1])).astype(jnp.bfloat16)
    whole_out = lax.all_gather(proj_out, "fs", axis=1, tiled=True)
    partial_value = matmul(gated_rows, whole_out)
    summed = lax.psum(partial_value.astype(jnp.bfloat16), "tp").astype(jnp.float32)
    stream_rows = (whole_tokens.astype(jnp.float32) + summed).astype(jnp.bfloat16)
    normed_two = local_rms(stream_rows, whole_ffn_gain)
    stream = lax.dynamic_slice_in_dim(stream_rows, lax.axis_index("tp") * own_width, own_width, 1)
    whole_gate, whole_value = (
        lax.all_gather(ffn_gate, "fs", axis=0, tiled=True),
        lax.all_gather(ffn_value, "fs", axis=0, tiled=True),
    )
    pre_gate = matmul(normed_two, whole_gate)
    pre_value = matmul(normed_two, whole_value)
    conv_g = causal_taps(pre_gate.astype(jnp.bfloat16), conv_gate)
    conv_v = causal_taps(pre_value.astype(jnp.bfloat16), conv_value)
    hidden = (jax.nn.silu(conv_g) * conv_v).astype(jnp.bfloat16)
    whole_down = lax.all_gather(proj_down, "fs", axis=1, tiled=True)
    partial_two = matmul(hidden, whole_down)
    return (
        stream.astype(jnp.float32)
        + lax.psum_scatter(
            partial_two.astype(jnp.bfloat16), "tp", scatter_dimension=1, tiled=True
        ).astype(jnp.float32)
    ).astype(jnp.bfloat16)


V, U, O, G, E, W = range(6)
BY_ROWS = (V, U, G, E)
VMEM_BYTES = 67043328


def gelu(values):
    return 0.5 * values * (1.0 + lax.erf(values * (0.5**0.5)))


def aligned(index, size):
    return pl.multiple_of(index * size, size)


def layer_kernel(
    fs_size,
    tokens,
    vectors,
    mix_weight,
    mix_bias,
    conv_gate,
    conv_value,
    proj_u,
    proj_v,
    proj_out,
    ffn_gate,
    ffn_value,
    proj_down,
    result,
    whole_v,
    whole_u,
    whole_out,
    whole_gate,
    whole_value,
    whole_down,
    rows_in,
    normed,
    gains,
    act_v,
    act_u,
    stat_cols,
    stat_own,
    stat_chip,
    stat_near,
    stat_far,
    masked,
    bias_cols,
    gated,
    partial,
    from_core,
    chip_sum,
    from_side,
    stream,
    pre_gate,
    hidden,
    total,
    near_down,
    far_down,
    local_sem,
    pool_send,
    pool_recv,
    ring_send,
    ring_recv,
    token_send,
    token_recv,
    stat_send,
    stat_recv,
    core_send,
    core_recv,
    side_send,
    side_recv,
    half_send,
    half_recv,
    near_send,
    near_recv,
    far_send,
    far_recv,
):
    pairs = fs_size // 2
    depth = pairs // 2
    last = 2 * (depth - 1)
    steps = last + 1
    index, core = lax.axis_index("fs"), lax.axis_index("tp")
    side, pair = index % 2, index // 2
    level, column = pair // 2, pair % 2
    spot = level * (1 - column) + (pairs - 1 - level) * column

    def pair_at(place):
        far = place // depth
        return 2 * (place * (1 - far) + (pairs - 1 - place) * far) + far

    def turned(shift):
        return pair_at((spot + shift + pairs) % pairs)

    right = (2 * turned(1) + side, core)
    left = (2 * turned(-1) + side, core)
    across = (2 * pair + 1 - side, core)
    partner = (index, 1 - core)

    own_rows, own_width = tokens.shape
    row_count, full = rows_in.shape
    tile = SEQ_LEN
    tiles = row_count // tile
    half_tiles = tiles // 2
    quarter = whole_v.shape[1]
    units = whole_gate.shape[1]
    groups = quarter // GROUP_DIM
    spread_width = 2 * 2 * quarter
    block_width = whole_out.shape[2]
    half_blocks = pairs // 2

    sources = (proj_v, proj_u, proj_out, ffn_gate, ffn_value, proj_down)
    wholes = (whole_v, whole_u, whole_out, whole_gate, whole_value, whole_down)

    def chunk(which, owner, part):
        whole = wholes[which]
        if which in BY_ROWS:
            depth_rows = sources[which].shape[0]
            return whole.at[pl.ds(aligned(2 * owner + part, depth_rows), depth_rows), :]
        width = sources[which].shape[1]
        return whole.at[owner, :, pl.ds(aligned(part, width), width)]

    def shard(which, part):
        source = sources[which]
        if which in BY_ROWS:
            width = source.shape[1] // 2
            return source.at[:, pl.ds(aligned(part, width), width)]
        height = source.shape[0] // 2
        return source.at[pl.ds(aligned(part, height), height), :]

    def remote(source, target, send, recv, device):
        return pltpu.make_async_remote_copy(
            src_ref=source,
            dst_ref=target,
            send_sem=send,
            recv_sem=recv,
            device_id=device,
            device_id_type=MESH,
        )

    def own_copy(which):
        return pltpu.make_async_copy(
            shard(which, side), chunk(which, pair, side), local_sem.at[which]
        )

    def pool_copy(which):
        return remote(
            shard(which, 1 - side),
            chunk(which, pair, side),
            pool_send.at[which],
            pool_recv.at[which],
            across,
        )

    def pool_arrived(which):
        here = chunk(which, pair, 1 - side)
        remote(here, here, pool_send.at[which], pool_recv.at[which], across).wait_recv()

    def relative(which_part):
        return side + which_part * (1 - 2 * side)

    def ring_copy(which, step, way, shift):
        part = step % 2 if way == 0 else step % 2 + step // last
        sign = 1 - 2 * way
        piece = chunk(which, turned(-sign * shift), relative(part))
        slot = (which * 2 + way) * steps + step
        return remote(
            piece, piece, ring_send.at[slot], ring_recv.at[slot], right if way == 0 else left
        )

    def ring_arrived(which, step, way):
        ring_copy(which, step, way, step // 2 + 1).wait_recv()

    def pump(which, step):
        if isinstance(step, int) and step == 0:
            own_copy(which).wait()
        elif isinstance(step, int) and step == 1:
            pool_arrived(which)
        else:
            ring_arrived(which, step - 2, 0)
            ring_arrived(which, step - 2 + step // last, 1)
        ring_copy(which, step, 0, step // 2).start()
        ring_copy(which, step, 1, step // 2).start()

    def drain(which):
        for step, way in ((last - 1, 0), (last, 0), (last - 2, 1), (last, 1)):
            ring_arrived(which, step, way)

    def token_region(which_side, which_core):
        return rows_in.at[
            pl.ds(aligned(which_side, own_rows), own_rows),
            pl.ds(aligned(which_core, own_width), own_width),
        ]

    def gain_region(which_core):
        return gains.at[:, pl.ds(aligned(which_core, own_width), own_width)]

    def token_copy(which, region, device):
        return remote(region, region, token_send.at[which], token_recv.at[which], device)

    def rows_of(place, height=tile):
        return pl.ds(aligned(place, height), height)

    barrier = pltpu.get_barrier_semaphore()
    for device in (right, left, across, partner):
        pl.semaphore_signal(barrier, inc=1, device_id=device, device_id_type=MESH)
    for which in (V, U):
        own_copy(which).start()
    tokens_in = pltpu.make_async_copy(tokens, token_region(side, core), local_sem.at[6])
    tokens_in.start()
    vectors_in = pltpu.make_async_copy(vectors, gain_region(core), local_sem.at[7])
    vectors_in.start()
    for which in (O, G, E, W):
        own_copy(which).start()
    pl.semaphore_wait(barrier, 4)

    for which in (V, U):
        pool_copy(which).start()
    for which in (V, U):
        pump(which, 0)
    tokens_in.wait()
    own_tokens = token_region(side, core)
    token_copy(0, own_tokens, across).start()
    token_copy(1, own_tokens, partner).start()
    vectors_in.wait()
    token_copy(3, gain_region(core), partner).start()
    for which in (O, G, E, W):
        pool_copy(which).start()
    for which in (V, U):
        pump(which, 1)

    head = side * groups
    above = lax.broadcasted_iota(jnp.int32, (BLOCK, BLOCK), 1)
    below = lax.broadcasted_iota(jnp.int32, (BLOCK, BLOCK), 0)
    visible = lax.div(above, SEGMENT) <= lax.div(below, SEGMENT)
    bias_rows = mix_bias[...].astype(jnp.float32)
    for group in range(groups):
        weight = mix_weight[head + group].astype(jnp.float32)
        masked[group] = jnp.where(visible, weight, 0.0).astype(jnp.bfloat16)
        lower, upper = bias_rows[group : group + 1], bias_rows[group + groups : group + groups + 1]
        row = jnp.where(side == 0, lower, upper)
        bias_cols[group] = jnp.broadcast_to(row, (LANES, BLOCK)).T

    def rms_tile(source, place, gain_index):
        step_rows = 32

        def one(part, carry):
            rows = pl.ds(aligned(place * (tile // step_rows) + part, step_rows), step_rows)
            values = source[rows, :].astype(jnp.float32)
            scale = lax.rsqrt(jnp.mean(values * values, axis=1, keepdims=True) + EPS)
            normed[rows, :] = (values * scale * gains[gain_index : gain_index + 1, :]).astype(
                jnp.bfloat16
            )
            return carry

        lax.fori_loop(0, tile // step_rows, one, 0)

    def product(target, rows, weights, width, finish):
        def one(part, carry):
            columns = pl.ds(aligned(part, width), width)
            value = jnp.dot(
                normed[rows, :], weights[:, columns], preferred_element_type=jnp.float32
            )
            target[rows, columns] = finish(value)
            return carry

        lax.fori_loop(0, weights.shape[1] // width, one, 0)

    token_copy(1, token_region(side, 1 - core), partner).wait_recv()
    token_copy(3, gain_region(1 - core), partner).wait_recv()
    for step in range(2, last):
        for which in (V, U):
            pump(which, step)
        if step - 2 < half_tiles:
            rms_tile(rows_in, side * half_tiles + step - 2, 0)
    token_copy(0, token_region(1 - side, core), across).wait_recv()
    token_copy(2, token_region(1 - side, core), partner).start()
    for which in (V, U):
        pump(which, last)
    pump(O, 0)
    pump(O, 1)
    pump(G, 0)
    token_copy(2, token_region(1 - side, 1 - core), partner).wait_recv()
    for place in range(half_tiles):
        rms_tile(rows_in, (1 - side) * half_tiles + place, 0)

    lane = lax.broadcasted_iota(jnp.int32, (64, LANES), 1)

    def act_tile(place, weights, target, with_stats):
        rows = rows_of(place)
        product(target, rows, weights, 256, lambda value: value)

        def one(part, carry):
            some = pl.ds(aligned(place * (tile // 64) + part, 64), 64)
            value = gelu(target[some, :])
            target[some, :] = value
            if with_stats:
                sums = jnp.sum(value, axis=1, keepdims=True)
                squares = jnp.sum(value * value, axis=1, keepdims=True)
                stat_cols[some, :] = jnp.where(lane == 0, sums, jnp.where(lane == 1, squares, 0.0))
            return carry

        lax.fori_loop(0, tile // 64, one, 0)
        if with_stats:
            for part in range(tile // LANES):
                some = pl.ds(aligned(place * (tile // LANES) + part, LANES), LANES)
                stat_own[:, some] = stat_cols[some, :].T[0:8, :]

    drain(V)

    def v_tile(place, carry):
        act_tile(place, whole_v, act_v, True)
        return carry

    lax.fori_loop(0, tiles, v_tile, 0)
    near_stats = remote(stat_own, stat_near, stat_send.at[0], stat_recv.at[0], partner)
    near_stats.start()
    for which, step in ((O, 2), (O, 3), (G, 1)):
        pump(which, step)
    near_stats.wait_recv()
    stat_chip[...] = stat_own[...] + stat_near[...]
    far_stats = remote(stat_chip, stat_far, stat_send.at[1], stat_recv.at[1], across)
    far_stats.start()
    drain(U)

    def u_tile(place, carry):
        act_tile(place, whole_u, act_u, False)
        return carry

    lax.fori_loop(0, tiles, u_tile, 0)
    for which, step in ((O, 4), (O, 5), (E, 0)):
        pump(which, step)
    far_stats.wait_recv()

    def mix_block(block, carry):
        rows = pl.ds(aligned(block, BLOCK), BLOCK)
        sums = stat_chip[0:2, rows] + stat_far[0:2, rows]
        center_row = sums[0:1] / spread_width
        spread_row = sums[1:2] / spread_width - center_row * center_row
        scale_row = lax.rsqrt(spread_row + EPS)
        center = jnp.broadcast_to(center_row, (LANES, BLOCK)).T
        scale = jnp.broadcast_to(scale_row, (LANES, BLOCK)).T
        for group in range(groups):
            columns = slice(group * GROUP_DIM, (group + 1) * GROUP_DIM)
            own = pl.ds(aligned(side * groups + group, GROUP_DIM), GROUP_DIM)
            mixed = (
                (act_v[rows, columns] - center) * scale * vectors[2:3, own] + vectors[3:4, own]
            ).astype(jnp.bfloat16)
            spatial = (
                jnp.dot(masked[group], mixed, preferred_element_type=jnp.float32)
                + bias_cols[group]
            )
            gated[rows, columns] = (act_u[rows, columns] * spatial).astype(jnp.bfloat16)
        return carry

    lax.fori_loop(0, row_count // BLOCK, mix_block, 0)
    pump(O, last)
    pump(E, 1)
    pump(G, 2)
    pump(G, 3)
    drain(O)

    own_columns = pl.ds(aligned(core, own_width), own_width)
    other_columns = pl.ds(aligned(1 - core, own_width), own_width)

    def core_copy(place):
        rows = rows_of(place)
        return remote(
            partial.at[rows, other_columns],
            from_core.at[rows, :],
            core_send.at[place],
            core_recv.at[place],
            partner,
        )

    def side_copy(place):
        rows = rows_of(place)
        return remote(
            chip_sum.at[rows, :],
            from_side.at[rows, :],
            side_send.at[place],
            side_recv.at[place],
            across,
        )

    def half_copy(place, columns):
        region = stream.at[rows_of(place), columns]
        return remote(region, region, half_send.at[place], half_recv.at[place], partner)

    def out_tile(place, carry):
        rows = rows_of(place)

        def one(block, inner):
            columns = pl.ds(aligned(block, block_width), block_width)
            value = jnp.dot(gated[rows, :], whole_out[block], preferred_element_type=jnp.float32)
            partial[rows, columns] = value.astype(jnp.bfloat16)
            return inner

        lax.fori_loop(0, pairs, one, 0)
        core_copy(place).start()
        return carry

    lax.fori_loop(0, tiles, out_tile, 0)

    def chip_tile(place, carry):
        core_copy(place).wait_recv()
        rows = rows_of(place)
        chip_sum[rows, :] = (
            partial[rows, own_columns].astype(jnp.float32)
            + from_core[rows, :].astype(jnp.float32)
        ).astype(jnp.bfloat16)
        side_copy(place).start()
        return carry

    lax.fori_loop(0, tiles, chip_tile, 0)

    def stream_tile(place):
        side_copy(place).wait_recv()
        rows = rows_of(place)
        stream[rows, own_columns] = (
            rows_in[rows, own_columns].astype(jnp.float32)
            + chip_sum[rows, :].astype(jnp.float32)
            + from_side[rows, :].astype(jnp.float32)
        ).astype(jnp.bfloat16)
        half_copy(place, own_columns).start()

    def to_bfloat(value):
        return value.astype(jnp.bfloat16)

    def gate_tile(place):
        half_copy(place, other_columns).wait_recv()
        rms_tile(stream, place, 1)
        product(pre_gate, rows_of(place), whole_gate, 256, to_bfloat)

    for which, step in ((G, 4), (G, 5), (G, 6)):
        pump(which, step)
    after_tiles = (((E, 2), (E, 3)), ((E, 4), (E, 5)), ((E, 6), (W, 0)), ((W, 1),))
    for place in range(tiles):
        stream_tile(place)
        for which, step in after_tiles[place]:
            pump(which, step)
        if place == 0:
            drain(G)
        gate_tile(place)

    drain(E)
    shifted = lax.broadcasted_iota(jnp.int32, (tile, 256), 0)

    def taps(values, weights):
        before = jnp.where(shifted >= 1, pltpu.roll(values, 1, 0), 0.0)
        earlier = jnp.where(shifted >= 2, pltpu.roll(values, 2, 0), 0.0)
        return earlier * weights[0:1] + before * weights[1:2] + values * weights[2:3]

    def value_tile(place):
        rows = rows_of(place)

        def one(part, carry):
            columns = pl.ds(aligned(part, 256), 256)
            own = pl.ds(aligned(side * (units // 256) + part, 256), 256)
            value = jnp.dot(
                normed[rows, :], whole_value[:, columns], preferred_element_type=jnp.float32
            )
            value = value.astype(jnp.bfloat16).astype(jnp.float32)
            gate = pre_gate[rows, columns].astype(jnp.float32)
            conv_g = taps(gate, conv_gate[:, own].astype(jnp.float32))
            conv_v = taps(value, conv_value[:, own].astype(jnp.float32))
            hidden[rows, columns] = (jax.nn.silu(conv_g) * conv_v).astype(jnp.bfloat16)
            return carry

        lax.fori_loop(0, units // 256, one, 0)

    def value_tiles(turn, carry):
        def one(place, inner):
            value_tile(2 * turn + place)
            return inner

        lax.fori_loop(0, 2, one, 0)
        pump(W, 2 + turn)
        return carry

    lax.fori_loop(0, tiles // 2, value_tiles, 0)

    given, kept = (1 - side), side

    def near_copy(order, block, which_side, which):
        rows = rows_of(which_side, own_rows)
        quarter_block = block % half_blocks
        return remote(
            partial.at[rows, pl.ds(aligned(block, block_width), block_width)],
            near_down.at[rows, pl.ds(aligned(quarter_block, block_width), block_width)],
            near_send.at[2 * order + which],
            near_recv.at[2 * order + which],
            partner,
        )

    def far_copy(order, block):
        columns = pl.ds(aligned(block % half_blocks, block_width), block_width)
        return remote(
            chip_sum.at[pl.ds(0, own_rows), columns],
            far_down.at[:, columns],
            far_send.at[order],
            far_recv.at[order],
            across,
        )

    def down_block(order, block):
        columns = pl.ds(aligned(block, block_width), block_width)
        for which, which_side in enumerate((given, kept)):

            def one(part, carry):
                rows = rows_of(which_side * half_tiles + part)
                value = jnp.dot(
                    hidden[rows, :], whole_down[block], preferred_element_type=jnp.float32
                )
                partial[rows, columns] = value.astype(jnp.bfloat16)
                return carry

            lax.fori_loop(0, half_tiles, one, 0)

            @pl.when(block // half_blocks != core)
            def _():
                near_copy(order, block, which_side, which).start()

    def down_sum(order, block):
        columns = pl.ds(aligned(block, block_width), block_width)
        quarter_columns = pl.ds(aligned(block % half_blocks, block_width), block_width)

        @pl.when(block // half_blocks == core)
        def _():
            near_copy(order, block, given, 0).wait_recv()
            rows = rows_of(given, own_rows)
            chip_sum[pl.ds(0, own_rows), quarter_columns] = (
                partial[rows, columns].astype(jnp.float32)
                + near_down[rows, quarter_columns].astype(jnp.float32)
            ).astype(jnp.bfloat16)
            far_copy(order, block).start()
            near_copy(order, block, kept, 1).wait_recv()
            rows = rows_of(kept, own_rows)
            total[:, quarter_columns] = (
                stream[rows, columns].astype(jnp.float32)
                + partial[rows, columns].astype(jnp.float32)
                + near_down[rows, quarter_columns].astype(jnp.float32)
            )

    def down_end(order, block):
        quarter_columns = pl.ds(aligned(block % half_blocks, block_width), block_width)

        @pl.when(block // half_blocks == core)
        def _():
            far_copy(order, block).wait_recv()
            result[:, quarter_columns] = (
                total[:, quarter_columns] + far_down[:, quarter_columns].astype(jnp.float32)
            ).astype(jnp.bfloat16)

    def sent(place, carry):
        core_copy(place).wait_send()
        side_copy(place).wait_send()
        half_copy(place, own_columns).wait_send()
        return carry

    lax.fori_loop(0, tiles, sent, 0)

    blocks = [turned(0)]
    down_block(0, blocks[0])
    down_sum(0, blocks[0])
    for hop in range(1, depth + 1):
        here = [turned(-hop), turned(hop)] if hop < depth else [turned(depth)]
        if hop < depth:
            ready = {0: (2 * hop - 2, 2 * hop - 1), 1: (2 * hop - 2, 2 * hop - 1)}
        else:
            ready = {0: (last,), 1: (last,)}
        forwarded = 2 + tiles // 2
        for step in range(2 * hop, min(2 * hop + 2, last + 1)):
            if step >= forwarded:
                pump(W, step)
        if hop == depth - 1:
            ring_arrived(W, last - 1, 0)
            ring_arrived(W, last - 2, 1)
        if hop == depth:
            ring_arrived(W, last, 0)
            ring_arrived(W, last, 1)
        for block in here:
            down_block(len(blocks), block)
            blocks.append(block)
        for order in range(len(blocks) - len(here), len(blocks)):
            down_sum(order, blocks[order])
    for order, block in enumerate(blocks):
        down_end(order, block)

    for which in range(6):
        for step in range(steps):
            for way in range(2):
                ring_copy(which, step, way, step // 2).wait_send()
        pool_copy(which).wait_send()
    for order, block in enumerate(blocks):

        @pl.when(block // half_blocks != core)
        def _():
            near_copy(order, block, given, 0).wait_send()
            near_copy(order, block, kept, 1).wait_send()

        @pl.when(block // half_blocks == core)
        def _():
            far_copy(order, block).wait_send()

    token_copy(0, own_tokens, across).wait_send()
    token_copy(1, own_tokens, partner).wait_send()
    token_copy(2, token_region(1 - side, core), partner).wait_send()
    token_copy(3, gain_region(core), partner).wait_send()
    near_stats.wait_send()
    far_stats.wait_send()


def on_ring(
    fs_size,
    tokens,
    norm_gain,
    proj_u,
    proj_v,
    layer_gain,
    layer_shift,
    mix_weight,
    mix_bias,
    proj_out,
    ffn_gain,
    ffn_gate,
    ffn_value,
    conv_gate,
    conv_value,
    proj_down,
):
    own_rows, own_width = tokens.shape
    row_count, full = 2 * own_rows, 2 * own_width
    pairs = fs_size // 2
    steps = 2 * (pairs // 2) - 1
    quarter, units = proj_u.shape[1] // 2, ffn_gate.shape[1] // 2
    groups = quarter // GROUP_DIM
    tiles = row_count // SEQ_LEN
    bf16, f32 = jnp.bfloat16, jnp.float32
    pack = jnp.stack([norm_gain, ffn_gain, layer_gain, layer_shift]).astype(f32)
    vectors = jnp.concatenate([pack, jnp.zeros_like(pack)], axis=0)
    vmem, hbm = pl.BlockSpec(memory_space=pltpu.VMEM), pl.BlockSpec(memory_space=pl.ANY)
    dma = pltpu.SemaphoreType.DMA
    scratch = [
        pltpu.VMEM((full, quarter), bf16),
        pltpu.VMEM((full, quarter), bf16),
        pltpu.VMEM((pairs, quarter, 2 * proj_out.shape[1]), bf16),
        pltpu.VMEM((full, units), bf16),
        pltpu.VMEM((full, units), bf16),
        pltpu.VMEM((pairs, units, 2 * proj_down.shape[1]), bf16),
        pltpu.VMEM((row_count, full), bf16),
        pltpu.VMEM((row_count, full), bf16),
        pltpu.VMEM((8, full), f32),
        pltpu.VMEM((row_count, quarter), f32),
        pltpu.VMEM((row_count, quarter), f32),
        pltpu.VMEM((row_count, LANES), f32),
        pltpu.VMEM((8, row_count), f32),
        pltpu.VMEM((8, row_count), f32),
        pltpu.VMEM((8, row_count), f32),
        pltpu.VMEM((8, row_count), f32),
        pltpu.VMEM((groups, BLOCK, BLOCK), bf16),
        pltpu.VMEM((groups, BLOCK, LANES), f32),
        pltpu.VMEM((row_count, quarter), bf16),
        pltpu.VMEM((row_count, full), bf16),
        pltpu.VMEM((row_count, own_width), bf16),
        pltpu.VMEM((row_count, own_width), bf16),
        pltpu.VMEM((row_count, own_width), bf16),
        pltpu.VMEM((row_count, full), bf16),
        pltpu.VMEM((row_count, units), bf16),
        pltpu.VMEM((row_count, units), bf16),
        pltpu.VMEM((own_rows, own_width), f32),
        pltpu.VMEM((row_count, own_width), bf16),
        pltpu.VMEM((own_rows, own_width), bf16),
        dma((8,)),
        dma((6,)),
        dma((6,)),
        dma((12 * steps,)),
        dma((12 * steps,)),
        dma((4,)),
        dma((4,)),
        dma((2,)),
        dma((2,)),
        dma((tiles,)),
        dma((tiles,)),
        dma((tiles,)),
        dma((tiles,)),
        dma((tiles,)),
        dma((tiles,)),
        dma((2 * pairs,)),
        dma((2 * pairs,)),
        dma((pairs,)),
        dma((pairs,)),
    ]
    return pl.pallas_call(
        functools.partial(layer_kernel, fs_size),
        out_shape=jax.ShapeDtypeStruct((own_rows, own_width), bf16),
        in_specs=[hbm, vmem, vmem, vmem, vmem, vmem] + [hbm] * 6,
        out_specs=vmem,
        scratch_shapes=scratch,
        compiler_params=pltpu.CompilerParams(
            collective_id=0, has_side_effects=True, vmem_limit_bytes=VMEM_BYTES
        ),
        name="layer",
    )(
        tokens,
        vectors,
        mix_weight,
        mix_bias,
        conv_gate,
        conv_value,
        proj_u,
        proj_v,
        proj_out,
        ffn_gate,
        ffn_value,
        proj_down,
    )


def solution(mesh):
    fs_size, tp_size = mesh.shape["fs"], mesh.shape["tp"]
    ringed = tp_size == 2 and fs_size == 16
    in_specs = (
        P("fs", "tp"),
        P("tp"),
        P("fs", "tp"),
        P("fs", "tp"),
        P("tp"),
        P("tp"),
        P("tp", None, None),
        P("tp", None),
        P("tp", "fs"),
        P("tp"),
        P("fs", "tp"),
        P("fs", "tp"),
        P(None, "tp"),
        P(None, "tp"),
        P("tp", "fs"),
    )
    return jax.shard_map(
        functools.partial(on_ring, fs_size) if ringed else on_device,
        mesh=mesh,
        in_specs=in_specs,
        out_specs=P("fs", "tp"),
        check_vma=False,
    )
```

profile of v0, /device:TPU:1, one launch (start us, length us, event | category | flops | bytes accessed | tf_op | source)
XLA Modules:
  0.0 201.2 jit_solution(12388132779652565016)
XLA Ops:
  0.0 0.0 copy-start
  0.0 0.7 stack.15
  0.7 0.0 copy-done
  0.7 0.0 copy-start.1
  0.7 0.7 copy-done.1
  1.4 0.0 copy-start.2
  1.4 0.7 copy-done.2
  2.1 0.6 fusion.7.vectors
  2.7 196.2 %layer.1 = bf16[512,1024]{1,0:T(8,128)(2,1)} custom-call(bf16[512,1024]{1,0:T(8,128)(2,1)} %tokens.1, f32[8,1024]{1,0:T(8,128)} %fusion.7.vectors, bf16[8,128,128]{2,1,0:T(8,128)(2,1)} %mix_weight.1, bf16[8,128]{1,0:T(8,128)(2,1)} %mix_bias.1, bf16[3,2048]{1,0:T(4,128)(2,1)} %conv_gate.1, bf16[3,2048]{1,0:T(4,128)(2,1)} %conv_value.1, ...), custom_call_target="tpu_custom_call" | custom-call | tf_op jit(solution)/shard_map/layer/pallas_call | solution.py:815
  199.0 2.3 %copy.17 = bf16[512,1024]{1,0:T(8,128)(2,1)} copy(bf16[512,1024]{1,0:T(8,128)(2,1)} %layer.1) | data formatting | bytes 2097152
  (3 shorter events, 0.0 us)
Async XLA Ops:
  0.0 0.7 copy-start
  0.7 0.7 copy-start.1
  1.4 0.7 copy-start.2
where the time goes:
time: 201 us
  Pallas kernels  196 us (98%)
  local copies, waits for them, and re-layouts  4.32 us (2%)
    pallas_call x1, Pallas kernels, on_ring(): pl.pallas_call(functools.partial(layer_kernel, fs_size), out_shape=jax.Sh...  196 us

commit v1 on v0

--- a/solution.py
+++ b/solution.py
@@ -122,6 +122,7 @@
 
 V, U, O, G, E, W = range(6)
 BY_ROWS = (V, U, G, E)
+GATING = (V, U, O)
 VMEM_BYTES = 67043328
 
 
@@ -182,6 +183,8 @@
     pool_recv,
     ring_send,
     ring_recv,
+    flow_send,
+    flow_recv,
     token_send,
     token_recv,
     stat_send,
@@ -192,6 +195,8 @@
     side_recv,
     half_send,
     half_recv,
+    depth_send,
+    depth_recv,
     near_send,
     near_recv,
     far_send,
@@ -217,6 +222,13 @@
     left = (2 * turned(-1) + side, core)
     across = (2 * pair + 1 - side, core)
     partner = (index, 1 - core)
+    plane = fs_size // 4
+    cell = index % plane
+    low, half = level % 2, level // 2
+    slot = (low + half) % 2
+    over = (index + 2 * (1 - 2 * column), core)
+    mate = (index + plane * (1 - 2 * low), core)
+    mirror = ((3 - level) * plane + cell, core)
 
     own_rows, own_width = tokens.shape
     row_count, full = rows_in.shape
@@ -249,6 +261,15 @@
         height = source.shape[0] // 2
         return source.at[pl.ds(aligned(part, height), height), :]
 
+    def piece(which, at_level, at_cell):
+        whole = wholes[which]
+        if which in BY_ROWS:
+            depth_rows = sources[which].shape[0]
+            return whole.at[pl.ds(aligned(at_level * plane + at_cell, depth_rows), depth_rows), :]
+        width = sources[which].shape[1]
+        block = (at_level // 2) * plane + at_cell
+        return whole.at[block, :, pl.ds(aligned(at_level % 2, width), width)]
+
     def remote(source, target, send, recv, device):
         return pltpu.make_async_remote_copy(
             src_ref=source,
@@ -260,22 +281,66 @@
         )
 
     def own_copy(which):
-        return pltpu.make_async_copy(
-            shard(which, side), chunk(which, pair, side), local_sem.at[which]
+        if which in GATING:
+            source, target = shard(which, side), chunk(which, pair, side)
+        else:
+            source, target = shard(which, slot), piece(which, level, cell)
+        return pltpu.make_async_copy(source, target, local_sem.at[which])
+
+    def pool_copy(which):
+        if which in GATING:
+            source, target, device = shard(which, 1 - side), chunk(which, pair, side), across
+        else:
+            source, target, device = shard(which, 1 - slot), piece(which, level, cell), mate
+        return remote(source, target, pool_send.at[which], pool_recv.at[which], device)
+
+    def pool_arrived(which):
+        if which in GATING:
+            here, device = chunk(which, pair, 1 - side), across
+        else:
+            here, device = piece(which, level + 1 - 2 * low, cell), mate
+        remote(here, here, pool_send.at[which], pool_recv.at[which], device).wait_recv()
+
+    facing = 3 - level
+    levels = (level, level + 1 - 2 * low, facing, facing + 1 - 2 * (facing % 2))
+    beside, beyond = cell + 1 - 2 * side, cell + 2 - 4 * column
+    across_diagonal = beside + 2 - 4 * column
+
+    def send_on(which, way, step):
+        if step < 4:
+            here = piece(which, levels[step], cell)
+        else:
+            here = piece(which, levels[2 * (step - 4) + way], (beyond, beside)[way])
+        place = (which - G) * 14 + way * 6 + step
+        return remote(
+            here, here, flow_send.at[place], flow_recv.at[place], (across, over)[way]
         )
 
-    def pool_copy(which):
-        return remote(
-            shard(which, 1 - side),
-            chunk(which, pair, side),
-            pool_send.at[which],
-            pool_recv.at[which],
-            across,
-        )
-
-    def pool_arrived(which):
-        here = chunk(which, pair, 1 - side)
-        remote(here, here, pool_send.at[which], pool_recv.at[which], across).wait_recv()
+    def come_in(which, way, step):
+        if step < 4:
+            here = piece(which, levels[step], (beside, beyond)[way])
+        else:
+            here = piece(which, levels[2 * (step - 4) + way], across_diagonal)
+        place = (which - G) * 14 + way * 6 + step
+        remote(
+            here, here, flow_send.at[place], flow_recv.at[place], (across, over)[way]
+        ).wait_recv()
+
+    def reflect(which, part):
+        here = piece(which, levels[part], cell)
+        place = (which - G) * 14 + 12 + part
+        return remote(here, here, flow_send.at[place], flow_recv.at[place], mirror)
+
+    def reflected(which, part):
+        here = piece(which, levels[2 + part], cell)
+        place = (which - G) * 14 + 12 + part
+        remote(here, here, flow_send.at[place], flow_recv.at[place], mirror).wait_recv()
+
+    def by_x(which, step):
+        send_on(which, 0, step).start()
+
+    def by_y(which, step):
+        send_on(which, 1, step).start()
 
     def relative(which_part):
         return side + which_part * (1 - 2 * side)
@@ -323,7 +388,7 @@
         return pl.ds(aligned(place, height), height)
 
     barrier = pltpu.get_barrier_semaphore()
-    for device in (right, left, across, partner):
+    for device in (right, left, across, over, mate, mirror, partner):
         pl.semaphore_signal(barrier, inc=1, device_id=device, device_id_type=MESH)
     for which in (V, U):
         own_copy(which).start()
@@ -333,7 +398,7 @@
     vectors_in.start()
     for which in (O, G, E, W):
         own_copy(which).start()
-    pl.semaphore_wait(barrier, 4)
+    pl.semaphore_wait(barrier, 7)
 
     for which in (V, U):
         pool_copy(which).start()
@@ -345,8 +410,10 @@
     token_copy(1, own_tokens, partner).start()
     vectors_in.wait()
     token_copy(3, gain_region(core), partner).start()
-    for which in (O, G, E, W):
-        pool_copy(which).start()
+    pool_copy(O).start()
+    for which in (G, E, W):
+        own_copy(which).wait()
+        by_x(which, 0)
     for which in (V, U):
         pump(which, 1)
 
@@ -400,7 +467,9 @@
         pump(which, last)
     pump(O, 0)
     pump(O, 1)
-    pump(G, 0)
+    pool_copy(G).start()
+    reflect(G, 0).start()
+    by_y(G, 0)
     token_copy(2, token_region(1 - side, 1 - core), partner).wait_recv()
     for place in range(half_tiles):
         rms_tile(rows_in, (1 - side) * half_tiles + place, 0)
@@ -436,8 +505,11 @@
     lax.fori_loop(0, tiles, v_tile, 0)
     near_stats = remote(stat_own, stat_near, stat_send.at[0], stat_recv.at[0], partner)
     near_stats.start()
-    for which, step in ((O, 2), (O, 3), (G, 1)):
-        pump(which, step)
+    pump(O, 2)
+    pump(O, 3)
+    pool_arrived(G)
+    reflect(G, 1).start()
+    by_x(G, 1)
     near_stats.wait_recv()
     stat_chip[...] = stat_own[...] + stat_near[...]
     far_stats = remote(stat_chip, stat_far, stat_send.at[1], stat_recv.at[1], across)
@@ -449,8 +521,11 @@
         return carry
 
     lax.fori_loop(0, tiles, u_tile, 0)
-    for which, step in ((O, 4), (O, 5), (E, 0)):
-        pump(which, step)
+    pump(O, 4)
+    pump(O, 5)
+    by_y(G, 1)
+    reflected(G, 0)
+    by_x(G, 2)
     far_stats.wait_recv()
 
     def mix_block(block, carry):
@@ -476,9 +551,11 @@
 
     lax.fori_loop(0, row_count // BLOCK, mix_block, 0)
     pump(O, last)
-    pump(E, 1)
-    pump(G, 2)
-    pump(G, 3)
+    by_y(G, 2)
+    pool_copy(E).start()
+    reflect(E, 0).start()
+    reflected(G, 1)
+    by_y(G, 3)
     drain(O)
 
     own_columns = pl.ds(aligned(core, own_width), own_width)
@@ -495,18 +572,24 @@
         )
 
     def side_copy(place):
-        rows = rows_of(place)
         return remote(
-            chip_sum.at[rows, :],
-            from_side.at[rows, :],
+            chip_sum.at[rows_of((1 - side) * half_tiles + place), :],
+            from_side.at[rows_of(place), :],
             side_send.at[place],
             side_recv.at[place],
             across,
         )
 
-    def half_copy(place, columns):
-        region = stream.at[rows_of(place), columns]
-        return remote(region, region, half_send.at[place], half_recv.at[place], partner)
+    def stream_rows(which_slot, place):
+        return rows_of(which_slot * half_tiles + place)
+
+    def half_copy(which_slot, place, columns, order):
+        region = stream.at[stream_rows(which_slot, place), columns]
+        return remote(region, region, half_send.at[order], half_recv.at[order], partner)
+
+    def depth_copy(which_slot, place):
+        region = stream.at[stream_rows(which_slot, place), own_columns]
+        return remote(region, region, depth_send.at[place], depth_recv.at[place], mate)
 
     def out_tile(place, carry):
         rows = rows_of(place)
@@ -521,50 +604,101 @@
         core_copy(place).start()
         return carry
 
-    lax.fori_loop(0, tiles, out_tile, 0)
-
-    def chip_tile(place, carry):
+    lax.fori_loop((1 - side) * half_tiles, (2 - side) * half_tiles, out_tile, 0)
+    lax.fori_loop(side * half_tiles, (1 + side) * half_tiles, out_tile, 0)
+
+    def chip_tile(place):
         core_copy(place).wait_recv()
         rows = rows_of(place)
         chip_sum[rows, :] = (
             partial[rows, own_columns].astype(jnp.float32)
             + from_core[rows, :].astype(jnp.float32)
         ).astype(jnp.bfloat16)
-        side_copy(place).start()
-        return carry
-
-    lax.fori_loop(0, tiles, chip_tile, 0)
-
-    def stream_tile(place):
+
+    def own_tile(place):
         side_copy(place).wait_recv()
-        rows = rows_of(place)
-        stream[rows, own_columns] = (
+        rows = rows_of(side * half_tiles + place)
+        stream[stream_rows(slot, place), own_columns] = (
             rows_in[rows, own_columns].astype(jnp.float32)
             + chip_sum[rows, :].astype(jnp.float32)
-            + from_side[rows, :].astype(jnp.float32)
+            + from_side[rows_of(place), :].astype(jnp.float32)
         ).astype(jnp.bfloat16)
-        half_copy(place, own_columns).start()
+        depth_copy(slot, place).start()
+        half_copy(slot, place, own_columns, place).start()
+
+    def far_tile(place):
+        depth_copy(1 - slot, place).wait_recv()
+        half_copy(1 - slot, place, own_columns, half_tiles + place).start()
 
     def to_bfloat(value):
         return value.astype(jnp.bfloat16)
 
-    def gate_tile(place):
-        half_copy(place, other_columns).wait_recv()
-        rms_tile(stream, place, 1)
-        product(pre_gate, rows_of(place), whole_gate, 256, to_bfloat)
-
-    for which, step in ((G, 4), (G, 5), (G, 6)):
-        pump(which, step)
-    after_tiles = (((E, 2), (E, 3)), ((E, 4), (E, 5)), ((E, 6), (W, 0)), ((W, 1),))
-    for place in range(tiles):
-        stream_tile(place)
-        for which, step in after_tiles[place]:
-            pump(which, step)
-        if place == 0:
-            drain(G)
-        gate_tile(place)
-
-    drain(E)
+    def gate_tile(which_slot, place, order):
+        half_copy(which_slot, place, other_columns, order).wait_recv()
+        rms_tile(stream, which_slot * half_tiles + place, 1)
+        product(pre_gate, stream_rows(which_slot, place), whole_gate, 256, to_bfloat)
+
+    come_in(G, 0, 1)
+    by_y(G, 4)
+    chip_tile((1 - side) * half_tiles)
+    side_copy(0).start()
+    by_x(G, 3)
+    for place in range(1, half_tiles):
+        chip_tile((1 - side) * half_tiles + place)
+        side_copy(place).start()
+    by_y(E, 0)
+    for place in range(half_tiles):
+        chip_tile(side * half_tiles + place)
+    come_in(G, 1, 0)
+    by_x(G, 4)
+    pool_arrived(E)
+    reflect(E, 1).start()
+    by_y(E, 1)
+    by_x(E, 1)
+    own_tile(0)
+    come_in(G, 0, 3)
+    by_y(G, 5)
+    come_in(G, 1, 2)
+    by_x(G, 5)
+    for place in range(1, half_tiles):
+        own_tile(place)
+    reflected(E, 0)
+    by_y(E, 2)
+    by_x(E, 2)
+    far_tile(0)
+    reflected(E, 1)
+    by_y(E, 3)
+    by_x(E, 3)
+    for step in (0, 2, 4, 5):
+        come_in(G, 0, step)
+    for step in (1, 3, 4, 5):
+        come_in(G, 1, step)
+    pool_copy(W).start()
+    reflect(W, 0).start()
+    gate_tile(slot, 0, 0)
+    gate_tile(slot, 1, 1)
+    come_in(E, 0, 1)
+    by_y(E, 4)
+    come_in(E, 1, 0)
+    by_x(E, 4)
+    for place in range(1, half_tiles):
+        far_tile(place)
+    gate_tile(1 - slot, 0, half_tiles)
+    come_in(E, 0, 3)
+    by_y(E, 5)
+    come_in(E, 1, 2)
+    by_x(E, 5)
+    by_y(W, 0)
+    pool_arrived(W)
+    reflect(W, 1).start()
+    by_y(W, 1)
+    by_x(W, 1)
+    for place in range(1, half_tiles):
+        gate_tile(1 - slot, place, half_tiles + place)
+    for step in (0, 2, 4, 5):
+        come_in(E, 0, step)
+    for step in (1, 3, 4, 5):
+        come_in(E, 1, step)
     shifted = lax.broadcasted_iota(jnp.int32, (tile, 256), 0)
 
     def taps(values, weights):
@@ -577,7 +711,7 @@
 
         def one(part, carry):
             columns = pl.ds(aligned(part, 256), 256)
-            own = pl.ds(aligned(side * (units // 256) + part, 256), 256)
+            own = pl.ds(aligned(slot * (units // 256) + part, 256), 256)
             value = jnp.dot(
                 normed[rows, :], whole_value[:, columns], preferred_element_type=jnp.float32
             )
@@ -591,17 +725,19 @@
         lax.fori_loop(0, units // 256, one, 0)
 
     def value_tiles(turn, carry):
-        def one(place, inner):
-            value_tile(2 * turn + place)
-            return inner
-
-        lax.fori_loop(0, 2, one, 0)
-        pump(W, 2 + turn)
+        value_tile(turn)
         return carry
 
-    lax.fori_loop(0, tiles // 2, value_tiles, 0)
-
-    given, kept = (1 - side), side
+    lax.fori_loop(0, half_tiles, value_tiles, 0)
+    reflected(W, 0)
+    by_y(W, 2)
+    by_x(W, 2)
+    lax.fori_loop(half_tiles, tiles, value_tiles, 0)
+    reflected(W, 1)
+    by_y(W, 3)
+    by_x(W, 3)
+
+    given, kept = (1 - slot), slot
 
     def near_copy(order, block, which_side, which):
         rows = rows_of(which_side, own_rows)
@@ -621,7 +757,7 @@
             far_down.at[:, columns],
             far_send.at[order],
             far_recv.at[order],
-            across,
+            mate,
         )
 
     def down_block(order, block):
@@ -657,11 +793,9 @@
             far_copy(order, block).start()
             near_copy(order, block, kept, 1).wait_recv()
             rows = rows_of(kept, own_rows)
-            total[:, quarter_columns] = (
-                stream[rows, columns].astype(jnp.float32)
-                + partial[rows, columns].astype(jnp.float32)
-                + near_down[rows, quarter_columns].astype(jnp.float32)
-            )
+            total[:, quarter_columns] = partial[rows, columns].astype(jnp.float32) + near_down[
+                rows, quarter_columns
+            ].astype(jnp.float32)
 
     def down_end(order, block):
         quarter_columns = pl.ds(aligned(block % half_blocks, block_width), block_width)
@@ -669,50 +803,75 @@
         @pl.when(block // half_blocks == core)
         def _():
             far_copy(order, block).wait_recv()
-            result[:, quarter_columns] = (
-                total[:, quarter_columns] + far_down[:, quarter_columns].astype(jnp.float32)
-            ).astype(jnp.bfloat16)
-
-    def sent(place, carry):
+            rows = rows_of(kept, own_rows)
+            strip_width = block_width // 2
+            for strip in range(2):
+                place = strip * plane + block % half_blocks
+                summed = pl.ds(aligned(2 * (block % half_blocks) + strip, strip_width), strip_width)
+                ours = pl.ds(aligned(core * 2 * plane + place, strip_width), strip_width)
+                result[:, pl.ds(aligned(place, strip_width), strip_width)] = (
+                    stream[rows, ours].astype(jnp.float32)
+                    + total[:, summed]
+                    + far_down[:, summed].astype(jnp.float32)
+                ).astype(jnp.bfloat16)
+
+    for place in range(tiles):
         core_copy(place).wait_send()
+    for place in range(half_tiles):
         side_copy(place).wait_send()
-        half_copy(place, own_columns).wait_send()
-        return carry
-
-    lax.fori_loop(0, tiles, sent, 0)
-
-    blocks = [turned(0)]
-    down_block(0, blocks[0])
-    down_sum(0, blocks[0])
-    for hop in range(1, depth + 1):
-        here = [turned(-hop), turned(hop)] if hop < depth else [turned(depth)]
-        if hop < depth:
-            ready = {0: (2 * hop - 2, 2 * hop - 1), 1: (2 * hop - 2, 2 * hop - 1)}
-        else:
-            ready = {0: (last,), 1: (last,)}
-        forwarded = 2 + tiles // 2
-        for step in range(2 * hop, min(2 * hop + 2, last + 1)):
-            if step >= forwarded:
-                pump(W, step)
-        if hop == depth - 1:
-            ring_arrived(W, last - 1, 0)
-            ring_arrived(W, last - 2, 1)
-        if hop == depth:
-            ring_arrived(W, last, 0)
-            ring_arrived(W, last, 1)
-        for block in here:
-            down_block(len(blocks), block)
-            blocks.append(block)
-        for order in range(len(blocks) - len(here), len(blocks)):
+
+    def block_at(at_level, at_cell):
+        return (at_level // 2) * plane + at_cell
+
+    cells = (cell, beside, beyond, across_diagonal)
+    blocks = [block_at(at_level, at_cell) for at_cell in cells for at_level in (level, facing)]
+
+    def run_blocks(*orders):
+        for order in orders:
+            down_block(order, blocks[order])
+        for order in orders:
             down_sum(order, blocks[order])
+
+    run_blocks(0, 1)
+    come_in(W, 0, 1)
+    by_y(W, 4)
+    come_in(W, 1, 0)
+    by_x(W, 4)
+    come_in(W, 0, 0)
+    come_in(W, 1, 1)
+    run_blocks(2, 4)
+    come_in(W, 0, 3)
+    by_y(W, 5)
+    come_in(W, 1, 2)
+    by_x(W, 5)
+    come_in(W, 0, 2)
+    come_in(W, 1, 3)
+    run_blocks(3, 5)
+    come_in(W, 0, 4)
+    come_in(W, 1, 4)
+    run_blocks(6)
+    come_in(W, 0, 5)
+    come_in(W, 1, 5)
+    run_blocks(7)
     for order, block in enumerate(blocks):
         down_end(order, block)
 
     for which in range(6):
-        for step in range(steps):
-            for way in range(2):
-                ring_copy(which, step, way, step // 2).wait_send()
+        if which in GATING:
+            for step in range(steps):
+                for way in range(2):
+                    ring_copy(which, step, way, step // 2).wait_send()
+        else:
+            for step in range(6):
+                for way in range(2):
+                    send_on(which, way, step).wait_send()
+            for part in range(2):
+                reflect(which, part).wait_send()
         pool_copy(which).wait_send()
+    for place in range(half_tiles):
+        depth_copy(slot, place).wait_send()
+        half_copy(slot, place, own_columns, place).wait_send()
+        half_copy(1 - slot, place, own_columns, half_tiles + place).wait_send()
     for order, block in enumerate(blocks):
 
         @pl.when(block // half_blocks != core)
@@ -785,7 +944,7 @@
         pltpu.VMEM((row_count, full), bf16),
         pltpu.VMEM((row_count, own_width), bf16),
         pltpu.VMEM((row_count, own_width), bf16),
-        pltpu.VMEM((row_count, own_width), bf16),
+        pltpu.VMEM((own_rows, own_width), bf16),
         pltpu.VMEM((row_count, full), bf16),
         pltpu.VMEM((row_count, units), bf16),
         pltpu.VMEM((row_count, units), bf16),
@@ -795,18 +954,22 @@
         dma((8,)),
         dma((6,)),
         dma((6,)),
-        dma((12 * steps,)),
-        dma((12 * steps,)),
+        dma((6 * steps,)),
+        dma((6 * steps,)),
+        dma((42,)),
+        dma((42,)),
         dma((4,)),
         dma((4,)),
         dma((2,)),
         dma((2,)),
         dma((tiles,)),
         dma((tiles,)),
+        dma((tiles // 2,)),
+        dma((tiles // 2,)),
         dma((tiles,)),
         dma((tiles,)),
-        dma((tiles,)),
-        dma((tiles,)),
+        dma((tiles // 2,)),
+        dma((tiles // 2,)),
         dma((2 * pairs,)),
         dma((2 * pairs,)),
         dma((pairs,)),

time: 201 us -> 219 us (1.090)
  Pallas kernels: 196 us -> 213 us
    pallas_call x1, Pallas kernels: 196 us -> 213 us  [on_ring(): pl.pallas_call(functools.partial(layer_kernel, fs_size), out_shape=jax.Sh...]
where the time goes in v1:
time: 219 us; the launch traced here: 218 us
  Pallas kernels  213 us (97%)
  local copies, waits for them, and re-layouts  4.32 us (2%)
    pallas_call x1, Pallas kernels, on_ring(): pl.pallas_call(functools.partial(layer_kernel, fs_size), out_shape=jax.Sh...  213 us

profile of v1, /device:TPU:1, one launch (start us, length us, event | category | flops | bytes accessed | tf_op | source)
XLA Modules:
  0.0 217.9 jit_solution(13053066501346694142)
XLA Ops:
  0.0 0.0 copy-start
  0.0 0.7 stack.15
  0.7 0.0 copy-done
  0.7 0.0 copy-start.1
  0.7 0.7 copy-done.1
  1.4 0.0 copy-start.2
  1.4 0.7 copy-done.2
  2.1 0.6 fusion.7.vectors
  2.7 213.0 %layer.1 = bf16[512,1024]{1,0:T(8,128)(2,1)} custom-call(bf16[512,1024]{1,0:T(8,128)(2,1)} %tokens.1, f32[8,1024]{1,0:T(8,128)} %fusion.7.vectors, bf16[8,128,128]{2,1,0:T(8,128)(2,1)} %mix_weight.1, bf16[8,128]{1,0:T(8,128)(2,1)} %mix_bias.1, bf16[3,2048]{1,0:T(4,128)(2,1)} %conv_gate.1, bf16[3,2048]{1,0:T(4,128)(2,1)} %conv_value.1, ...), custom_call_target="tpu_custom_call" | custom-call | tf_op jit(solution)/shard_map/layer/pallas_call | solution.py:978
  215.7 2.3 %copy.17 = bf16[512,1024]{1,0:T(8,128)(2,1)} copy(bf16[512,1024]{1,0:T(8,128)(2,1)} %layer.1) | data formatting | bytes 2097152
  (3 shorter events, 0.0 us)
Async XLA Ops:
  0.0 0.7 copy-start
  0.7 0.7 copy-start.1
  1.4 0.7 copy-start.2

commit v2 on v0

--- a/solution.py
+++ b/solution.py
@@ -121,6 +121,24 @@
 
 
 V, U, O, G, E, W = range(6)
+NAMES = ("V", "U", "O", "G", "E", "W")
+ORDER = (
+    "yG0", "poolG", "yV0", "poolU", "xG0", "xO0", "poolV", "yO0", "poolE", "xU0", "poolO",
+    "halftok", "yW0", "poolW", "mirV0", "yU0", "mirO0", "yE0", "mirG0", "xG4", "xV4", "yG1", "xG1",
+    "mirV1", "xV1", "mirU0", "mirU1", "mirO1", "prep", "xE0", "yU1", "xO4", "yE1", "xV2", "xV0",
+    "yO1", "yV2", "xO1", "yG2", "Nk1", "xV3", "xV5", "Nk0", "tok", "mirG1", "xU2", "yO2", "mirE0",
+    "xU1", "yU3", "yU2", "xU3", "yV5", "xO5", "xO2", "yV1", "mirE1", "xU4", "yO4", "mirW1", "xO3",
+    "xG2", "xU5", "yV3", "yU5", "yV4", "fwd", "Ng0", "yO5", "Ng1", "yU4", "yO3", "Vk1", "xE1",
+    "Vk0", "xG5", "yE2", "Vg1", "xG3", "Vg0", "statA", "yG4", "yG3", "statB", "xE2", "yE4", "statC",
+    "Uk1", "Mk1", "Ok1", "Uk0", "Mk0", "xE3", "xE4", "mirW0", "Ck1", "sidek1", "yG5", "xE5", "Ug0",
+    "Ug1", "Ok0", "Ck0", "Mg1", "xW0", "yW2", "sidek0", "Og1", "Cg1", "yE5", "Sg1", "Gg1", "xW2",
+    "sideg1", "Mg0", "yE3", "yW1", "yW3", "Og0", "Cg0", "sideg0", "Sg0", "xW3", "Gg0", "Eg0", "xW1",
+    "Eg1", "DG4", "DG5", "DG0", "Sk1", "DG2", "SG2", "Gk1", "xW4", "SG4", "far4", "yW4", "Ek1",
+    "DG6", "SG0", "yW5", "Sk0", "far2", "SG6", "xW5", "far6", "SG5", "far5", "Gk0", "Ek0", "far0",
+    "DK5", "DG3", "DG1", "DK7", "SG1", "DG7", "DK2", "far1", "DK4", "SK7", "DK6", "SK4", "SG7",
+    "far7", "END4", "SG3", "far3", "DK0", "SK2", "END2", "DK3", "DK1", "END7", "SK1", "END1", "SK0",
+    "END0", "SK6", "END6", "SK5", "END5", "SK3", "END3",
+)
 BY_ROWS = (V, U, G, E)
 VMEM_BYTES = 67043328
 
@@ -175,13 +193,14 @@
     pre_gate,
     hidden,
     total,
+    given_down,
     near_down,
     far_down,
     local_sem,
     pool_send,
     pool_recv,
-    ring_send,
-    ring_recv,
+    flow_send,
+    flow_recv,
     token_send,
     token_recv,
     stat_send,
@@ -198,25 +217,22 @@
     far_recv,
 ):
     pairs = fs_size // 2
-    depth = pairs // 2
-    last = 2 * (depth - 1)
-    steps = last + 1
+    plane = fs_size // 4
     index, core = lax.axis_index("fs"), lax.axis_index("tp")
-    side, pair = index % 2, index // 2
-    level, column = pair // 2, pair % 2
-    spot = level * (1 - column) + (pairs - 1 - level) * column
-
-    def pair_at(place):
-        far = place // depth
-        return 2 * (place * (1 - far) + (pairs - 1 - place) * far) + far
-
-    def turned(shift):
-        return pair_at((spot + shift + pairs) % pairs)
-
-    right = (2 * turned(1) + side, core)
-    left = (2 * turned(-1) + side, core)
-    across = (2 * pair + 1 - side, core)
+    level, cell = index // plane, index % plane
+    side, column = cell % 2, cell // 2
+    low, half = level % 2, level // 2
+    slot = (low + half) % 2
+    facing = 3 - level
+    levels = (level, level + 1 - 2 * low, facing, facing + 1 - 2 * (facing % 2))
+    beside, beyond = cell + 1 - 2 * side, cell + 2 - 4 * column
+    diagonal = beside + 2 - 4 * column
+
     partner = (index, 1 - core)
+    mate = (levels[1] * plane + cell, core)
+    mirror = (facing * plane + cell, core)
+    across = (level * plane + beside, core)
+    over = (level * plane + beyond, core)
 
     own_rows, own_width = tokens.shape
     row_count, full = rows_in.shape
@@ -233,14 +249,6 @@
     sources = (proj_v, proj_u, proj_out, ffn_gate, ffn_value, proj_down)
     wholes = (whole_v, whole_u, whole_out, whole_gate, whole_value, whole_down)
 
-    def chunk(which, owner, part):
-        whole = wholes[which]
-        if which in BY_ROWS:
-            depth_rows = sources[which].shape[0]
-            return whole.at[pl.ds(aligned(2 * owner + part, depth_rows), depth_rows), :]
-        width = sources[which].shape[1]
-        return whole.at[owner, :, pl.ds(aligned(part, width), width)]
-
     def shard(which, part):
         source = sources[which]
         if which in BY_ROWS:
@@ -248,6 +256,15 @@
             return source.at[:, pl.ds(aligned(part, width), width)]
         height = source.shape[0] // 2
         return source.at[pl.ds(aligned(part, height), height), :]
+
+    def piece(which, at_level, at_cell):
+        whole = wholes[which]
+        if which in BY_ROWS:
+            depth_rows = sources[which].shape[0]
+            return whole.at[pl.ds(aligned(at_level * plane + at_cell, depth_rows), depth_rows), :]
+        width = sources[which].shape[1]
+        block = (at_level // 2) * plane + at_cell
+        return whole.at[block, :, pl.ds(aligned(at_level % 2, width), width)]
 
     def remote(source, target, send, recv, device):
         return pltpu.make_async_remote_copy(
@@ -261,51 +278,45 @@
 
     def own_copy(which):
         return pltpu.make_async_copy(
-            shard(which, side), chunk(which, pair, side), local_sem.at[which]
+            shard(which, slot), piece(which, level, cell), local_sem.at[which]
         )
 
     def pool_copy(which):
         return remote(
-            shard(which, 1 - side),
-            chunk(which, pair, side),
+            shard(which, 1 - slot),
+            piece(which, level, cell),
             pool_send.at[which],
             pool_recv.at[which],
-            across,
+            mate,
         )
 
     def pool_arrived(which):
-        here = chunk(which, pair, 1 - side)
-        remote(here, here, pool_send.at[which], pool_recv.at[which], across).wait_recv()
-
-    def relative(which_part):
-        return side + which_part * (1 - 2 * side)
-
-    def ring_copy(which, step, way, shift):
-        part = step % 2 if way == 0 else step % 2 + step // last
-        sign = 1 - 2 * way
-        piece = chunk(which, turned(-sign * shift), relative(part))
-        slot = (which * 2 + way) * steps + step
-        return remote(
-            piece, piece, ring_send.at[slot], ring_recv.at[slot], right if way == 0 else left
-        )
-
-    def ring_arrived(which, step, way):
-        ring_copy(which, step, way, step // 2 + 1).wait_recv()
-
-    def pump(which, step):
-        if isinstance(step, int) and step == 0:
-            own_copy(which).wait()
-        elif isinstance(step, int) and step == 1:
-            pool_arrived(which)
+        here = piece(which, levels[1], cell)
+        remote(here, here, pool_send.at[which], pool_recv.at[which], mate).wait_recv()
+
+    def moved(which, here, slot_index, device):
+        place = which * 14 + slot_index
+        return remote(here, here, flow_send.at[place], flow_recv.at[place], device)
+
+    def send_on(which, way, step):
+        if step < 4:
+            here = piece(which, levels[step], cell)
         else:
-            ring_arrived(which, step - 2, 0)
-            ring_arrived(which, step - 2 + step // last, 1)
-        ring_copy(which, step, 0, step // 2).start()
-        ring_copy(which, step, 1, step // 2).start()
-
-    def drain(which):
-        for step, way in ((last - 1, 0), (last, 0), (last - 2, 1), (last, 1)):
-            ring_arrived(which, step, way)
+            here = piece(which, levels[2 * (step - 4) + way], (beyond, beside)[way])
+        return moved(which, here, way * 6 + step, (across, over)[way])
+
+    def come_in(which, way, step):
+        if step < 4:
+            here = piece(which, levels[step], (beside, beyond)[way])
+        else:
+            here = piece(which, levels[2 * (step - 4) + way], diagonal)
+        moved(which, here, way * 6 + step, (across, over)[way]).wait_recv()
+
+    def reflect(which, part):
+        return moved(which, piece(which, levels[part], cell), 12 + part, mirror)
+
+    def reflected(which, part):
+        moved(which, piece(which, levels[2 + part], cell), 12 + part, mirror).wait_recv()
 
     def token_region(which_side, which_core):
         return rows_in.at[
@@ -323,44 +334,104 @@
         return pl.ds(aligned(place, height), height)
 
     barrier = pltpu.get_barrier_semaphore()
-    for device in (right, left, across, partner):
+    for device in (across, over, mate, mirror, partner):
         pl.semaphore_signal(barrier, inc=1, device_id=device, device_id_type=MESH)
-    for which in (V, U):
+    for which in (V, U, O):
         own_copy(which).start()
-    tokens_in = pltpu.make_async_copy(tokens, token_region(side, core), local_sem.at[6])
+    tokens_in = pltpu.make_async_copy(tokens, token_region(slot, core), local_sem.at[6])
     tokens_in.start()
     vectors_in = pltpu.make_async_copy(vectors, gain_region(core), local_sem.at[7])
     vectors_in.start()
-    for which in (O, G, E, W):
+    for which in (G, E, W):
         own_copy(which).start()
-    pl.semaphore_wait(barrier, 4)
-
-    for which in (V, U):
-        pool_copy(which).start()
-    for which in (V, U):
-        pump(which, 0)
+    pl.semaphore_wait(barrier, 5)
+
+    own_tokens = token_region(slot, core)
+    def arrive_pool(which):
+        return lambda: pool_arrived(which)
+
+    def arrive_mirror(which, part):
+        return lambda: reflected(which, part)
+
+    def arrive_flow(which, way, step):
+        return lambda: come_in(which, way, step)
+
+    done = set()
+
+    def once(name, wait):
+        if name not in done:
+            done.add(name)
+            wait()
+
+    def own_here(which):
+        once(("own", which), lambda: own_copy(which).wait())
+
+    def pool_here(which):
+        once(("pool", which), arrive_pool(which))
+
+    def mirror_here(which, part):
+        once(("mirror", which, part), arrive_mirror(which, part))
+
+    def flow_here(which, way, step):
+        once(("flow", which, way, step), arrive_flow(which, way, step))
+
+    def part_here(which, part):
+        (own_here, pool_here)[part](which)
+
+    def all_here(which):
+        own_here(which)
+        pool_here(which)
+        for part in range(2):
+            mirror_here(which, part)
+        for step in range(6):
+            for way in range(2):
+                flow_here(which, way, step)
+
+    def send_flow(which, way, step):
+        if step < 2:
+            part_here(which, step)
+        elif step < 4:
+            mirror_here(which, step - 2)
+        else:
+            flow_here(which, 1 - way, 2 * (step - 4) + way)
+        send_on(which, way, step).start()
+
+    def send_mirror(which, part):
+        part_here(which, part)
+        reflect(which, part).start()
+
     tokens_in.wait()
-    own_tokens = token_region(side, core)
-    token_copy(0, own_tokens, across).start()
     token_copy(1, own_tokens, partner).start()
     vectors_in.wait()
     token_copy(3, gain_region(core), partner).start()
-    for which in (O, G, E, W):
-        pool_copy(which).start()
-    for which in (V, U):
-        pump(which, 1)
-
-    head = side * groups
-    above = lax.broadcasted_iota(jnp.int32, (BLOCK, BLOCK), 1)
-    below = lax.broadcasted_iota(jnp.int32, (BLOCK, BLOCK), 0)
-    visible = lax.div(above, SEGMENT) <= lax.div(below, SEGMENT)
-    bias_rows = mix_bias[...].astype(jnp.float32)
-    for group in range(groups):
-        weight = mix_weight[head + group].astype(jnp.float32)
-        masked[group] = jnp.where(visible, weight, 0.0).astype(jnp.bfloat16)
-        lower, upper = bias_rows[group : group + 1], bias_rows[group + groups : group + groups + 1]
-        row = jnp.where(side == 0, lower, upper)
-        bias_cols[group] = jnp.broadcast_to(row, (LANES, BLOCK)).T
+
+    head = slot * groups
+
+    def prepare():
+        above = lax.broadcasted_iota(jnp.int32, (BLOCK, BLOCK), 1)
+        below = lax.broadcasted_iota(jnp.int32, (BLOCK, BLOCK), 0)
+        visible = lax.div(above, SEGMENT) <= lax.div(below, SEGMENT)
+        bias_rows = mix_bias[...].astype(jnp.float32)
+        for group in range(groups):
+            weight = mix_weight[head + group].astype(jnp.float32)
+            masked[group] = jnp.where(visible, weight, 0.0).astype(jnp.bfloat16)
+            lower = bias_rows[group : group + 1]
+            upper = bias_rows[group + groups : group + groups + 1]
+            row = jnp.where(slot == 0, lower, upper)
+            bias_cols[group] = jnp.broadcast_to(row, (LANES, BLOCK)).T
+
+    first, second = slot * half_tiles, (1 - slot) * half_tiles
+
+    def near_tokens():
+        token_copy(1, token_region(slot, 1 - core), partner).wait_recv()
+        token_copy(3, gain_region(1 - core), partner).wait_recv()
+
+    def pass_tokens():
+        token_copy(0, token_region(1 - slot, core), mate).wait_recv()
+        token_copy(2, token_region(1 - slot, core), partner).start()
+
+    def last_tokens():
+        token_copy(2, token_region(1 - slot, 1 - core), partner).wait_recv()
 
     def rms_tile(source, place, gain_index):
         step_rows = 32
@@ -386,24 +457,6 @@
             return carry
 
         lax.fori_loop(0, weights.shape[1] // width, one, 0)
-
-    token_copy(1, token_region(side, 1 - core), partner).wait_recv()
-    token_copy(3, gain_region(1 - core), partner).wait_recv()
-    for step in range(2, last):
-        for which in (V, U):
-            pump(which, step)
-        if step - 2 < half_tiles:
-            rms_tile(rows_in, side * half_tiles + step - 2, 0)
-    token_copy(0, token_region(1 - side, core), across).wait_recv()
-    token_copy(2, token_region(1 - side, core), partner).start()
-    for which in (V, U):
-        pump(which, last)
-    pump(O, 0)
-    pump(O, 1)
-    pump(G, 0)
-    token_copy(2, token_region(1 - side, 1 - core), partner).wait_recv()
-    for place in range(half_tiles):
-        rms_tile(rows_in, (1 - side) * half_tiles + place, 0)
 
     lane = lax.broadcasted_iota(jnp.int32, (64, LANES), 1)
 
@@ -427,31 +480,12 @@
                 some = pl.ds(aligned(place * (tile // LANES) + part, LANES), LANES)
                 stat_own[:, some] = stat_cols[some, :].T[0:8, :]
 
-    drain(V)
-
-    def v_tile(place, carry):
-        act_tile(place, whole_v, act_v, True)
-        return carry
-
-    lax.fori_loop(0, tiles, v_tile, 0)
     near_stats = remote(stat_own, stat_near, stat_send.at[0], stat_recv.at[0], partner)
-    near_stats.start()
-    for which, step in ((O, 2), (O, 3), (G, 1)):
-        pump(which, step)
-    near_stats.wait_recv()
-    stat_chip[...] = stat_own[...] + stat_near[...]
-    far_stats = remote(stat_chip, stat_far, stat_send.at[1], stat_recv.at[1], across)
-    far_stats.start()
-    drain(U)
-
-    def u_tile(place, carry):
-        act_tile(place, whole_u, act_u, False)
-        return carry
-
-    lax.fori_loop(0, tiles, u_tile, 0)
-    for which, step in ((O, 4), (O, 5), (E, 0)):
-        pump(which, step)
-    far_stats.wait_recv()
+    far_stats = remote(stat_chip, stat_far, stat_send.at[1], stat_recv.at[1], mate)
+
+    def sum_stats():
+        near_stats.wait_recv()
+        stat_chip[...] = stat_own[...] + stat_near[...]
 
     def mix_block(block, carry):
         rows = pl.ds(aligned(block, BLOCK), BLOCK)
@@ -463,7 +497,7 @@
         scale = jnp.broadcast_to(scale_row, (LANES, BLOCK)).T
         for group in range(groups):
             columns = slice(group * GROUP_DIM, (group + 1) * GROUP_DIM)
-            own = pl.ds(aligned(side * groups + group, GROUP_DIM), GROUP_DIM)
+            own = pl.ds(aligned(slot * groups + group, GROUP_DIM), GROUP_DIM)
             mixed = (
                 (act_v[rows, columns] - center) * scale * vectors[2:3, own] + vectors[3:4, own]
             ).astype(jnp.bfloat16)
@@ -474,12 +508,10 @@
             gated[rows, columns] = (act_u[rows, columns] * spatial).astype(jnp.bfloat16)
         return carry
 
-    lax.fori_loop(0, row_count // BLOCK, mix_block, 0)
-    pump(O, last)
-    pump(E, 1)
-    pump(G, 2)
-    pump(G, 3)
-    drain(O)
+    def mix_tile(place):
+        once("stats", far_stats.wait_recv)
+        ratio = tile // BLOCK
+        lax.fori_loop(place * ratio, (place + 1) * ratio, mix_block, 0)
 
     own_columns = pl.ds(aligned(core, own_width), own_width)
     other_columns = pl.ds(aligned(1 - core, own_width), own_width)
@@ -501,14 +533,14 @@
             from_side.at[rows, :],
             side_send.at[place],
             side_recv.at[place],
-            across,
+            mate,
         )
 
     def half_copy(place, columns):
         region = stream.at[rows_of(place), columns]
         return remote(region, region, half_send.at[place], half_recv.at[place], partner)
 
-    def out_tile(place, carry):
+    def out_tile(place):
         rows = rows_of(place)
 
         def one(block, inner):
@@ -519,30 +551,35 @@
 
         lax.fori_loop(0, pairs, one, 0)
         core_copy(place).start()
-        return carry
-
-    lax.fori_loop(0, tiles, out_tile, 0)
-
-    def chip_tile(place, carry):
+
+    def chip_tile(place):
         core_copy(place).wait_recv()
         rows = rows_of(place)
         chip_sum[rows, :] = (
             partial[rows, own_columns].astype(jnp.float32)
             + from_core[rows, :].astype(jnp.float32)
         ).astype(jnp.bfloat16)
-        side_copy(place).start()
-        return carry
-
-    lax.fori_loop(0, tiles, chip_tile, 0)
+
+    strip_width = block_width // 2
+
+    def strips():
+        for strip in range(2):
+            for place in range(half_blocks):
+                ours = pl.ds(
+                    aligned(core * 2 * plane + strip * plane + place, strip_width), strip_width
+                )
+                start = (2 * place + strip) * strip_width
+                yield ours, slice(start, start + strip_width)
 
     def stream_tile(place):
         side_copy(place).wait_recv()
         rows = rows_of(place)
-        stream[rows, own_columns] = (
-            rows_in[rows, own_columns].astype(jnp.float32)
-            + chip_sum[rows, :].astype(jnp.float32)
-            + from_side[rows, :].astype(jnp.float32)
-        ).astype(jnp.bfloat16)
+        for ours, summed in strips():
+            stream[rows, ours] = (
+                rows_in[rows, ours].astype(jnp.float32)
+                + chip_sum[rows, summed].astype(jnp.float32)
+                + from_side[rows, summed].astype(jnp.float32)
+            ).astype(jnp.bfloat16)
         half_copy(place, own_columns).start()
 
     def to_bfloat(value):
@@ -553,18 +590,6 @@
         rms_tile(stream, place, 1)
         product(pre_gate, rows_of(place), whole_gate, 256, to_bfloat)
 
-    for which, step in ((G, 4), (G, 5), (G, 6)):
-        pump(which, step)
-    after_tiles = (((E, 2), (E, 3)), ((E, 4), (E, 5)), ((E, 6), (W, 0)), ((W, 1),))
-    for place in range(tiles):
-        stream_tile(place)
-        for which, step in after_tiles[place]:
-            pump(which, step)
-        if place == 0:
-            drain(G)
-        gate_tile(place)
-
-    drain(E)
     shifted = lax.broadcasted_iota(jnp.int32, (tile, 256), 0)
 
     def taps(values, weights):
@@ -577,7 +602,7 @@
 
         def one(part, carry):
             columns = pl.ds(aligned(part, 256), 256)
-            own = pl.ds(aligned(side * (units // 256) + part, 256), 256)
+            own = pl.ds(aligned(slot * (units // 256) + part, 256), 256)
             value = jnp.dot(
                 normed[rows, :], whole_value[:, columns], preferred_element_type=jnp.float32
             )
@@ -590,18 +615,7 @@
 
         lax.fori_loop(0, units // 256, one, 0)
 
-    def value_tiles(turn, carry):
-        def one(place, inner):
-            value_tile(2 * turn + place)
-            return inner
-
-        lax.fori_loop(0, 2, one, 0)
-        pump(W, 2 + turn)
-        return carry
-
-    lax.fori_loop(0, tiles // 2, value_tiles, 0)
-
-    given, kept = (1 - side), side
+    given, kept = (1 - slot), slot
 
     def near_copy(order, block, which_side, which):
         rows = rows_of(which_side, own_rows)
@@ -617,32 +631,32 @@
     def far_copy(order, block):
         columns = pl.ds(aligned(block % half_blocks, block_width), block_width)
         return remote(
-            chip_sum.at[pl.ds(0, own_rows), columns],
+            given_down.at[:, columns],
             far_down.at[:, columns],
             far_send.at[order],
             far_recv.at[order],
-            across,
+            mate,
         )
 
-    def down_block(order, block):
+    def down_block(order, which):
+        block = blocks[order]
+        which_side = (given, kept)[which]
         columns = pl.ds(aligned(block, block_width), block_width)
-        for which, which_side in enumerate((given, kept)):
-
-            def one(part, carry):
-                rows = rows_of(which_side * half_tiles + part)
-                value = jnp.dot(
-                    hidden[rows, :], whole_down[block], preferred_element_type=jnp.float32
-                )
-                partial[rows, columns] = value.astype(jnp.bfloat16)
-                return carry
-
-            lax.fori_loop(0, half_tiles, one, 0)
-
-            @pl.when(block // half_blocks != core)
-            def _():
-                near_copy(order, block, which_side, which).start()
-
-    def down_sum(order, block):
+
+        def one(part, carry):
+            rows = rows_of(which_side * half_tiles + part)
+            value = jnp.dot(hidden[rows, :], whole_down[block], preferred_element_type=jnp.float32)
+            partial[rows, columns] = value.astype(jnp.bfloat16)
+            return carry
+
+        lax.fori_loop(0, half_tiles, one, 0)
+
+        @pl.when(block // half_blocks != core)
+        def _():
+            near_copy(order, block, which_side, which).start()
+
+    def given_sum(order):
+        block = blocks[order]
         columns = pl.ds(aligned(block, block_width), block_width)
         quarter_columns = pl.ds(aligned(block % half_blocks, block_width), block_width)
 
@@ -650,18 +664,30 @@
         def _():
             near_copy(order, block, given, 0).wait_recv()
             rows = rows_of(given, own_rows)
-            chip_sum[pl.ds(0, own_rows), quarter_columns] = (
+            given_down[:, quarter_columns] = (
                 partial[rows, columns].astype(jnp.float32)
                 + near_down[rows, quarter_columns].astype(jnp.float32)
             ).astype(jnp.bfloat16)
+
+    def send_given(order):
+        block = blocks[order]
+
+        @pl.when(block // half_blocks == core)
+        def _():
             far_copy(order, block).start()
+
+    def kept_sum(order):
+        block = blocks[order]
+        columns = pl.ds(aligned(block, block_width), block_width)
+        quarter_columns = pl.ds(aligned(block % half_blocks, block_width), block_width)
+
+        @pl.when(block // half_blocks == core)
+        def _():
             near_copy(order, block, kept, 1).wait_recv()
             rows = rows_of(kept, own_rows)
-            total[:, quarter_columns] = (
-                stream[rows, columns].astype(jnp.float32)
-                + partial[rows, columns].astype(jnp.float32)
-                + near_down[rows, quarter_columns].astype(jnp.float32)
-            )
+            total[:, quarter_columns] = partial[rows, columns].astype(jnp.float32) + near_down[
+                rows, quarter_columns
+            ].astype(jnp.float32)
 
     def down_end(order, block):
         quarter_columns = pl.ds(aligned(block % half_blocks, block_width), block_width)
@@ -669,50 +695,114 @@
         @pl.when(block // half_blocks == core)
         def _():
             far_copy(order, block).wait_recv()
-            result[:, quarter_columns] = (
-                total[:, quarter_columns] + far_down[:, quarter_columns].astype(jnp.float32)
-            ).astype(jnp.bfloat16)
-
-    def sent(place, carry):
-        core_copy(place).wait_send()
+            rows = rows_of(kept, own_rows)
+            for strip in range(2):
+                place = strip * plane + block % half_blocks
+                summed = pl.ds(aligned(2 * (block % half_blocks) + strip, strip_width), strip_width)
+                ours = pl.ds(aligned(core * 2 * plane + place, strip_width), strip_width)
+                result[:, pl.ds(aligned(place, strip_width), strip_width)] = (
+                    stream[rows, ours].astype(jnp.float32)
+                    + total[:, summed]
+                    + far_down[:, summed].astype(jnp.float32)
+                ).astype(jnp.bfloat16)
+
+    def block_at(at_level, at_cell):
+        return (at_level // 2) * plane + at_cell
+
+    cells = (cell, beside, beyond, diagonal)
+    blocks = [block_at(at_level, at_cell) for at_level in (level, facing) for at_cell in cells]
+
+    needed = (
+        (("pool",),),
+        (("x", 0), ("x", 1)),
+        (("y", 0), ("y", 1)),
+        (("x", 4), ("y", 4)),
+        (("mirror", 0), ("mirror", 1)),
+        (("x", 2), ("x", 3)),
+        (("y", 2), ("y", 3)),
+        (("x", 5), ("y", 5)),
+    )
+
+    def block_here(order):
+        for kind, *rest in needed[order]:
+            if kind == "pool":
+                own_here(W)
+                pool_here(W)
+            elif kind == "mirror":
+                mirror_here(W, rest[0])
+            else:
+                flow_here(W, ("x", "y").index(kind), rest[0])
+
+    def share_block(order, which):
+        for place in range(tiles):
+            once(("core", place), core_copy(place).wait_send)
+        block_here(order)
+        down_block(order, which)
+
+    tile_steps = {
+        "N": lambda place: rms_tile(rows_in, place, 0),
+        "V": lambda place: act_tile(place, whole_v, act_v, True),
+        "U": lambda place: act_tile(place, whole_u, act_u, False),
+        "M": mix_tile,
+        "O": out_tile,
+        "C": chip_tile,
+        "side": lambda place: side_copy(place).start(),
+        "S": stream_tile,
+        "G": gate_tile,
+        "E": value_tile,
+    }
+    plain_steps = {
+        "prep": prepare,
+        "tok": lambda: token_copy(0, own_tokens, mate).start(),
+        "halftok": near_tokens,
+        "fwd": pass_tokens,
+        "statA": near_stats.start,
+        "statB": sum_stats,
+        "statC": far_stats.start,
+    }
+    block_steps = {
+        "DG": lambda order: share_block(order, 0),
+        "SG": given_sum,
+        "far": send_given,
+        "DK": lambda order: share_block(order, 1),
+        "SK": kept_sum,
+        "END": lambda order: down_end(order, blocks[order]),
+    }
+    uses = {"V": V, "U": U, "O": O, "G": G, "E": E}
+
+    def run_step(name):
+        stem, tail = name[:-2], name[-2:]
+        if name in plain_steps:
+            plain_steps[name]()
+        elif stem in tile_steps and tail[0] in "kg":
+            if stem in uses:
+                all_here(uses[stem])
+            if stem == "N" and tail[0] == "g":
+                once("tokens", last_tokens)
+            tile_steps[stem]((first if tail[0] == "k" else second) + int(tail[1]))
+        elif name[:-1] in block_steps:
+            block_steps[name[:-1]](int(name[-1]))
+        elif name[:4] == "pool":
+            pool_copy(NAMES.index(name[4])).start()
+        elif name[:3] == "mir":
+            send_mirror(NAMES.index(name[3]), int(name[4]))
+        else:
+            send_flow(NAMES.index(name[1]), ("x", "y").index(name[0]), int(name[2]))
+
+    for name in ORDER:
+        run_step(name)
+
+    for place in range(tiles):
         side_copy(place).wait_send()
+    for which in range(6):
+        for step in range(6):
+            for way in range(2):
+                send_on(which, way, step).wait_send()
+        for part in range(2):
+            reflect(which, part).wait_send()
+        pool_copy(which).wait_send()
+    for place in range(tiles):
         half_copy(place, own_columns).wait_send()
-        return carry
-
-    lax.fori_loop(0, tiles, sent, 0)
-
-    blocks = [turned(0)]
-    down_block(0, blocks[0])
-    down_sum(0, blocks[0])
-    for hop in range(1, depth + 1):
-        here = [turned(-hop), turned(hop)] if hop < depth else [turned(depth)]
-        if hop < depth:
-            ready = {0: (2 * hop - 2, 2 * hop - 1), 1: (2 * hop - 2, 2 * hop - 1)}
-        else:
-            ready = {0: (last,), 1: (last,)}
-        forwarded = 2 + tiles // 2
-        for step in range(2 * hop, min(2 * hop + 2, last + 1)):
-            if step >= forwarded:
-                pump(W, step)
-        if hop == depth - 1:
-            ring_arrived(W, last - 1, 0)
-            ring_arrived(W, last - 2, 1)
-        if hop == depth:
-            ring_arrived(W, last, 0)
-            ring_arrived(W, last, 1)
-        for block in here:
-            down_block(len(blocks), block)
-            blocks.append(block)
-        for order in range(len(blocks) - len(here), len(blocks)):
-            down_sum(order, blocks[order])
-    for order, block in enumerate(blocks):
-        down_end(order, block)
-
-    for which in range(6):
-        for step in range(steps):
-            for way in range(2):
-                ring_copy(which, step, way, step // 2).wait_send()
-        pool_copy(which).wait_send()
     for order, block in enumerate(blocks):
 
         @pl.when(block // half_blocks != core)
@@ -724,9 +814,9 @@
         def _():
             far_copy(order, block).wait_send()
 
-    token_copy(0, own_tokens, across).wait_send()
+    token_copy(0, own_tokens, mate).wait_send()
     token_copy(1, own_tokens, partner).wait_send()
-    token_copy(2, token_region(1 - side, core), partner).wait_send()
+    token_copy(2, token_region(1 - slot, core), partner).wait_send()
     token_copy(3, gain_region(core), partner).wait_send()
     near_stats.wait_send()
     far_stats.wait_send()
@@ -753,7 +843,6 @@
     own_rows, own_width = tokens.shape
     row_count, full = 2 * own_rows, 2 * own_width
     pairs = fs_size // 2
-    steps = 2 * (pairs // 2) - 1
     quarter, units = proj_u.shape[1] // 2, ffn_gate.shape[1] // 2
     groups = quarter // GROUP_DIM
     tiles = row_count // SEQ_LEN
@@ -790,13 +879,14 @@
         pltpu.VMEM((row_count, units), bf16),
         pltpu.VMEM((row_count, units), bf16),
         pltpu.VMEM((own_rows, own_width), f32),
+        pltpu.VMEM((own_rows, own_width), bf16),
         pltpu.VMEM((row_count, own_width), bf16),
         pltpu.VMEM((own_rows, own_width), bf16),
         dma((8,)),
         dma((6,)),
         dma((6,)),
-        dma((12 * steps,)),
-        dma((12 * steps,)),
+        dma((84,)),
+        dma((84,)),
         dma((4,)),
         dma((4,)),
         dma((2,)),

time: 201 us -> 190 us (0.945)
  Pallas kernels: 196 us -> 184 us
    pallas_call x1, Pallas kernels: 196 us -> 184 us  [on_ring(): pl.pallas_call(functools.partial(layer_kernel, fs_size), out_shape=jax.Sh...]
where the time goes in v2:
time: 190 us; the launch traced here: 189 us
  Pallas kernels  184 us (97%)
  local copies, waits for them, and re-layouts  4.32 us (2%)
    pallas_call x1, Pallas kernels, on_ring(): pl.pallas_call(functools.partial(layer_kernel, fs_size), out_shape=jax.Sh...  184 us

profile of v2, /device:TPU:1, one launch (start us, length us, event | category | flops | bytes accessed | tf_op | source)
XLA Modules:
  0.0 189.2 jit_solution(6638595379067381232)
XLA Ops:
  0.0 0.0 copy-start
  0.0 0.7 stack.15
  0.7 0.0 copy-done
  0.7 0.0 copy-start.1
  0.7 0.7 copy-done.1
  1.4 0.0 copy-start.2
  1.4 0.7 copy-done.2
  2.1 0.6 fusion.7.vectors
  2.7 184.2 %layer.1 = bf16[512,1024]{1,0:T(8,128)(2,1)} custom-call(bf16[512,1024]{1,0:T(8,128)(2,1)} %tokens.1, f32[8,1024]{1,0:T(8,128)} %fusion.7.vectors, bf16[8,128,128]{2,1,0:T(8,128)(2,1)} %mix_weight.1, bf16[8,128]{1,0:T(8,128)(2,1)} %mix_bias.1, bf16[3,2048]{1,0:T(4,128)(2,1)} %conv_gate.1, bf16[3,2048]{1,0:T(4,128)(2,1)} %conv_value.1, ...), custom_call_target="tpu_custom_call" | custom-call | tf_op jit(solution)/shard_map/layer/pallas_call | solution.py:905
  186.9 2.3 %copy.17 = bf16[512,1024]{1,0:T(8,128)(2,1)} copy(bf16[512,1024]{1,0:T(8,128)(2,1)} %layer.1) | data formatting | bytes 2097152
  (3 shorter events, 0.0 us)
Async XLA Ops:
  0.0 0.7 copy-start
  0.7 0.7 copy-start.1
  1.4 0.7 copy-start.2

commit v3 on v2

--- a/solution.py
+++ b/solution.py
@@ -123,21 +123,21 @@
 V, U, O, G, E, W = range(6)
 NAMES = ("V", "U", "O", "G", "E", "W")
 ORDER = (
-    "yG0", "poolG", "yV0", "poolU", "xG0", "xO0", "poolV", "yO0", "poolE", "xU0", "poolO",
-    "halftok", "yW0", "poolW", "mirV0", "yU0", "mirO0", "yE0", "mirG0", "xG4", "xV4", "yG1", "xG1",
-    "mirV1", "xV1", "mirU0", "mirU1", "mirO1", "prep", "xE0", "yU1", "xO4", "yE1", "xV2", "xV0",
-    "yO1", "yV2", "xO1", "yG2", "Nk1", "xV3", "xV5", "Nk0", "tok", "mirG1", "xU2", "yO2", "mirE0",
-    "xU1", "yU3", "yU2", "xU3", "yV5", "xO5", "xO2", "yV1", "mirE1", "xU4", "yO4", "mirW1", "xO3",
-    "xG2", "xU5", "yV3", "yU5", "yV4", "fwd", "Ng0", "yO5", "Ng1", "yU4", "yO3", "Vk1", "xE1",
-    "Vk0", "xG5", "yE2", "Vg1", "xG3", "Vg0", "statA", "yG4", "yG3", "statB", "xE2", "yE4", "statC",
-    "Uk1", "Mk1", "Ok1", "Uk0", "Mk0", "xE3", "xE4", "mirW0", "Ck1", "sidek1", "yG5", "xE5", "Ug0",
-    "Ug1", "Ok0", "Ck0", "Mg1", "xW0", "yW2", "sidek0", "Og1", "Cg1", "yE5", "Sg1", "Gg1", "xW2",
-    "sideg1", "Mg0", "yE3", "yW1", "yW3", "Og0", "Cg0", "sideg0", "Sg0", "xW3", "Gg0", "Eg0", "xW1",
-    "Eg1", "DG4", "DG5", "DG0", "Sk1", "DG2", "SG2", "Gk1", "xW4", "SG4", "far4", "yW4", "Ek1",
-    "DG6", "SG0", "yW5", "Sk0", "far2", "SG6", "xW5", "far6", "SG5", "far5", "Gk0", "Ek0", "far0",
-    "DK5", "DG3", "DG1", "DK7", "SG1", "DG7", "DK2", "far1", "DK4", "SK7", "DK6", "SK4", "SG7",
-    "far7", "END4", "SG3", "far3", "DK0", "SK2", "END2", "DK3", "DK1", "END7", "SK1", "END1", "SK0",
-    "END0", "SK6", "END6", "SK5", "END5", "SK3", "END3",
+    "poolO", "poolU", "poolE", "poolV", "yV0", "poolG", "xV0", "poolW", "xW0", "mirV0", "mirU0",
+    "yU0", "xU4", "xO1", "xO0", "yW0", "mirE0", "yO1", "mirO1", "yE1", "mirU1", "prep", "mirO0",
+    "xV1", "xV4", "xU1", "mirV1", "yU1", "yO0", "yG0", "yG1", "yV4", "halftok", "xU0", "xG1", "xU2",
+    "yV1", "xG4", "yV2", "xE0", "xU3", "yU2", "xV5", "tok", "mirG1", "xV3", "mirW0", "xO3", "xE1",
+    "xG0", "Nk0", "yO3", "mirG0", "Nk1", "yV3", "yV5", "yO2", "yU4", "xO4", "yU3", "yU5", "mirE1",
+    "yE0", "yE2", "fwd", "xU5", "xV2", "Ng1", "yO5", "xO2", "yO4", "xO5", "Vk0", "yG4", "xG3",
+    "Ng0", "Vg1", "xE4", "Vg0", "Vk1", "statA", "Ug1", "statB", "statC", "Uk1", "xG2", "yG2", "Mk1",
+    "Ok1", "yG5", "Uk0", "xW2", "yG3", "mirW1", "xE3", "Ck1", "sidek1", "Mg1", "yE3", "Ug0", "xG5",
+    "Mg0", "Og1", "Cg1", "xE2", "Mk0", "Ok0", "Ck0", "sidek0", "Sg1", "yE5", "sideg1", "xE5", "Og0",
+    "Gg1", "yE4", "yW2", "xW1", "Cg0", "yW1", "Sg0", "Gg0", "Eg0", "sideg0", "xW3", "yW3", "Eg1",
+    "DG0", "xW5", "xW4", "DG4", "Sk1", "SG4", "far4", "DG1", "SG1", "SG0", "far0", "Gk1", "yW4",
+    "DG2", "Ek1", "DG5", "SG5", "SG2", "yW5", "Sk0", "far5", "far2", "DG6", "Gk0", "Ek0", "DK0",
+    "SG6", "far6", "DG3", "DK6", "SG3", "DG7", "far3", "DK2", "SG7", "DK5", "far1", "DK4", "SK5",
+    "SK2", "DK3", "far7", "END2", "SK0", "END0", "SK4", "DK7", "END4", "SK3", "END3", "SK6", "END5",
+    "DK1", "SK1", "END1", "END6", "SK7", "END7",
 )
 BY_ROWS = (V, U, G, E)
 VMEM_BYTES = 67043328
@@ -154,7 +154,10 @@
 def layer_kernel(
     fs_size,
     tokens,
-    vectors,
+    norm_gain,
+    ffn_gain,
+    layer_gain,
+    layer_shift,
     mix_weight,
     mix_bias,
     conv_gate,
@@ -196,6 +199,7 @@
     given_down,
     near_down,
     far_down,
+    finished,
     local_sem,
     pool_send,
     pool_recv,
@@ -215,6 +219,7 @@
     near_recv,
     far_send,
     far_recv,
+    out_sem,
 ):
     pairs = fs_size // 2
     plane = fs_size // 4
@@ -340,10 +345,11 @@
         own_copy(which).start()
     tokens_in = pltpu.make_async_copy(tokens, token_region(slot, core), local_sem.at[6])
     tokens_in.start()
-    vectors_in = pltpu.make_async_copy(vectors, gain_region(core), local_sem.at[7])
-    vectors_in.start()
     for which in (G, E, W):
         own_copy(which).start()
+    for row, vector in enumerate((norm_gain, ffn_gain, layer_gain, layer_shift)):
+        values = vector[...].astype(jnp.float32).reshape(1, own_width)
+        gains[row : row + 1, pl.ds(aligned(core, own_width), own_width)] = values
     pl.semaphore_wait(barrier, 5)
 
     own_tokens = token_region(slot, core)
@@ -402,7 +408,6 @@
 
     tokens_in.wait()
     token_copy(1, own_tokens, partner).start()
-    vectors_in.wait()
     token_copy(3, gain_region(core), partner).start()
 
     head = slot * groups
@@ -497,9 +502,9 @@
         scale = jnp.broadcast_to(scale_row, (LANES, BLOCK)).T
         for group in range(groups):
             columns = slice(group * GROUP_DIM, (group + 1) * GROUP_DIM)
-            own = pl.ds(aligned(slot * groups + group, GROUP_DIM), GROUP_DIM)
+            own = pl.ds(aligned((core * 2 + slot) * groups + group, GROUP_DIM), GROUP_DIM)
             mixed = (
-                (act_v[rows, columns] - center) * scale * vectors[2:3, own] + vectors[3:4, own]
+                (act_v[rows, columns] - center) * scale * gains[2:3, own] + gains[3:4, own]
             ).astype(jnp.bfloat16)
             spatial = (
                 jnp.dot(masked[group], mixed, preferred_element_type=jnp.float32)
@@ -689,6 +694,14 @@
                 rows, quarter_columns
             ].astype(jnp.float32)
 
+    def strip_out(order, strip, block):
+        columns = pl.ds(
+            aligned(strip * plane + block % half_blocks, block_width // 2), block_width // 2
+        )
+        return pltpu.make_async_copy(
+            finished.at[:, columns], result.at[:, columns], out_sem.at[2 * order + strip]
+        )
+
     def down_end(order, block):
         quarter_columns = pl.ds(aligned(block % half_blocks, block_width), block_width)
 
@@ -700,11 +713,12 @@
                 place = strip * plane + block % half_blocks
                 summed = pl.ds(aligned(2 * (block % half_blocks) + strip, strip_width), strip_width)
                 ours = pl.ds(aligned(core * 2 * plane + place, strip_width), strip_width)
-                result[:, pl.ds(aligned(place, strip_width), strip_width)] = (
+                finished[:, pl.ds(aligned(place, strip_width), strip_width)] = (
                     stream[rows, ours].astype(jnp.float32)
                     + total[:, summed]
                     + far_down[:, summed].astype(jnp.float32)
                 ).astype(jnp.bfloat16)
+                strip_out(order, strip, block).start()
 
     def block_at(at_level, at_cell):
         return (at_level // 2) * plane + at_cell
@@ -733,9 +747,12 @@
             else:
                 flow_here(W, ("x", "y").index(kind), rest[0])
 
+    def core_sent(place):
+        core_copy(place).wait_send()
+
     def share_block(order, which):
         for place in range(tiles):
-            once(("core", place), core_copy(place).wait_send)
+            once(("core", place), functools.partial(core_sent, place))
         block_here(order)
         down_block(order, which)
 
@@ -813,6 +830,8 @@
         @pl.when(block // half_blocks == core)
         def _():
             far_copy(order, block).wait_send()
+            for strip in range(2):
+                strip_out(order, strip, block).wait()
 
     token_copy(0, own_tokens, mate).wait_send()
     token_copy(1, own_tokens, partner).wait_send()
@@ -847,8 +866,6 @@
     groups = quarter // GROUP_DIM
     tiles = row_count // SEQ_LEN
     bf16, f32 = jnp.bfloat16, jnp.float32
-    pack = jnp.stack([norm_gain, ffn_gain, layer_gain, layer_shift]).astype(f32)
-    vectors = jnp.concatenate([pack, jnp.zeros_like(pack)], axis=0)
     vmem, hbm = pl.BlockSpec(memory_space=pltpu.VMEM), pl.BlockSpec(memory_space=pl.ANY)
     dma = pltpu.SemaphoreType.DMA
     scratch = [
@@ -882,6 +899,7 @@
         pltpu.VMEM((own_rows, own_width), bf16),
         pltpu.VMEM((row_count, own_width), bf16),
         pltpu.VMEM((own_rows, own_width), bf16),
+        pltpu.VMEM((own_rows, own_width), bf16),
         dma((8,)),
         dma((6,)),
         dma((6,)),
@@ -901,12 +919,13 @@
         dma((2 * pairs,)),
         dma((pairs,)),
         dma((pairs,)),
+        dma((2 * pairs,)),
     ]
     return pl.pallas_call(
         functools.partial(layer_kernel, fs_size),
         out_shape=jax.ShapeDtypeStruct((own_rows, own_width), bf16),
-        in_specs=[hbm, vmem, vmem, vmem, vmem, vmem] + [hbm] * 6,
-        out_specs=vmem,
+        in_specs=[hbm] + [vmem] * 8 + [hbm] * 6,
+        out_specs=hbm,
         scratch_shapes=scratch,
         compiler_params=pltpu.CompilerParams(
             collective_id=0, has_side_effects=True, vmem_limit_bytes=VMEM_BYTES
@@ -914,7 +933,10 @@
         name="layer",
     )(
         tokens,
-        vectors,
+        norm_gain,
+        ffn_gain,
+        layer_gain,
+        layer_shift,
         mix_weight,
         mix_bias,
         conv_gate,

time: 190 us -> 186 us (0.979)
  local copies, waits for them, and re-layouts: 4.32 us -> 2.26 us
where the time goes in v3:
time: 186 us; the launch traced here: 185 us
  Pallas kernels  183 us (98%)
  local copies, waits for them, and re-layouts  2.26 us (1%)
    pallas_call x1, Pallas kernels, on_ring(): pl.pallas_call(functools.partial(layer_kernel, fs_size), out_shape=jax.Sh...  183 us

profile of v3, /device:TPU:1, one launch (start us, length us, event | category | flops | bytes accessed | tf_op | source)
XLA Modules:
  0.0 185.4 jit_solution(13688887807990707217)
XLA Ops:
  0.0 183.1 %layer.1 = bf16[512,1024]{1,0:T(8,128)(2,1)} custom-call(bf16[512,1024]{1,0:T(8,128)(2,1)} %tokens.1, bf16[1024]{0:T(1024)(128)(2,1)} %norm_gain.1, bf16[1024]{0:T(1024)(128)(2,1)} %ffn_gain.1, bf16[1024]{0:T(1024)(128)(2,1)} %layer_gain.1, bf16[1024]{0:T(1024)(128)(2,1)} %layer_shift.1, bf16[8,128,128]{2,1,0:T(8,128)(2,1)} %mix_weight.1, ...), custom_call_target="tpu_custom_call" | custom-call | tf_op jit(solution)/shard_map/layer/pallas_call | solution.py:924
  183.1 2.3 %copy.17 = bf16[512,1024]{1,0:T(8,128)(2,1)} copy(bf16[512,1024]{1,0:T(8,128)(2,1)} %layer.1) | data formatting | bytes 2097152

commit v4 on v3

--- a/solution.py
+++ b/solution.py
@@ -123,21 +123,21 @@
 V, U, O, G, E, W = range(6)
 NAMES = ("V", "U", "O", "G", "E", "W")
 ORDER = (
-    "poolO", "poolU", "poolE", "poolV", "yV0", "poolG", "xV0", "poolW", "xW0", "mirV0", "mirU0",
-    "yU0", "xU4", "xO1", "xO0", "yW0", "mirE0", "yO1", "mirO1", "yE1", "mirU1", "prep", "mirO0",
-    "xV1", "xV4", "xU1", "mirV1", "yU1", "yO0", "yG0", "yG1", "yV4", "halftok", "xU0", "xG1", "xU2",
-    "yV1", "xG4", "yV2", "xE0", "xU3", "yU2", "xV5", "tok", "mirG1", "xV3", "mirW0", "xO3", "xE1",
-    "xG0", "Nk0", "yO3", "mirG0", "Nk1", "yV3", "yV5", "yO2", "yU4", "xO4", "yU3", "yU5", "mirE1",
-    "yE0", "yE2", "fwd", "xU5", "xV2", "Ng1", "yO5", "xO2", "yO4", "xO5", "Vk0", "yG4", "xG3",
-    "Ng0", "Vg1", "xE4", "Vg0", "Vk1", "statA", "Ug1", "statB", "statC", "Uk1", "xG2", "yG2", "Mk1",
-    "Ok1", "yG5", "Uk0", "xW2", "yG3", "mirW1", "xE3", "Ck1", "sidek1", "Mg1", "yE3", "Ug0", "xG5",
-    "Mg0", "Og1", "Cg1", "xE2", "Mk0", "Ok0", "Ck0", "sidek0", "Sg1", "yE5", "sideg1", "xE5", "Og0",
-    "Gg1", "yE4", "yW2", "xW1", "Cg0", "yW1", "Sg0", "Gg0", "Eg0", "sideg0", "xW3", "yW3", "Eg1",
-    "DG0", "xW5", "xW4", "DG4", "Sk1", "SG4", "far4", "DG1", "SG1", "SG0", "far0", "Gk1", "yW4",
-    "DG2", "Ek1", "DG5", "SG5", "SG2", "yW5", "Sk0", "far5", "far2", "DG6", "Gk0", "Ek0", "DK0",
-    "SG6", "far6", "DG3", "DK6", "SG3", "DG7", "far3", "DK2", "SG7", "DK5", "far1", "DK4", "SK5",
-    "SK2", "DK3", "far7", "END2", "SK0", "END0", "SK4", "DK7", "END4", "SK3", "END3", "SK6", "END5",
-    "DK1", "SK1", "END1", "END6", "SK7", "END7",
+    "yV0", "xG0", "xO0", "yE0", "yG0", "yW0", "poolU", "mirU0", "mirU1", "xU1", "poolV", "xE4",
+    "mirV1", "xV0", "mirV0", "crsV", "poolG", "xV1", "crsU", "crsO", "yU2", "halftok", "poolO",
+    "mirO0", "xU2", "yU0", "yO0", "yV3", "yU4", "xV3", "prep", "Nk0", "crsG", "yV1", "mirO1", "xV4",
+    "xV2", "yU1", "mirE0", "xO4", "xU5", "Nk1", "yV5", "yU3", "yV2", "xU3", "xG1", "poolE", "mirE1",
+    "tok", "poolW", "xU0", "yO1", "yG4", "xV5", "xO3", "mirG0", "xU4", "xO1", "yV4", "yO2", "mirG1",
+    "xG4", "yU5", "xE1", "yG1", "fwd", "Vk1", "xO2", "yO3", "Ng1", "crsE", "Ug1", "yO5", "xE2",
+    "Uk0", "Uk1", "Vg1", "Vk0", "xO5", "Ng0", "yO4", "Vg0", "statA", "statB", "statC", "xG2", "yE4",
+    "Mk0", "yG2", "crsW", "yE1", "xG3", "mirW0", "Ug0", "Mg0", "Mk1", "Ok1", "Ck1", "sidek1", "xE0",
+    "Og0", "yG3", "Cg0", "sideg0", "yE3", "yG5", "Mg1", "Og1", "yE2", "xG5", "xW1", "Cg1", "Ok0",
+    "xE3", "yE5", "Ck0", "Sg1", "sidek0", "yW1", "xW0", "xE5", "Sk0", "Gk0", "yW4", "yW2", "mirW1",
+    "Gg1", "xW4", "sideg1", "Sg0", "xW2", "Gg0", "Eg0", "Eg1", "DG2", "DG1", "DG0", "SG0", "SG2",
+    "far0", "Sk1", "xW3", "DG3", "SG1", "far1", "xW5", "DG4", "far2", "yW3", "Gk1", "yW5", "SG4",
+    "far4", "SG3", "far3", "Ek0", "Ek1", "DK2", "DK1", "DG6", "DG5", "SG6", "far6", "DK0", "SK1",
+    "DG7", "SG5", "far5", "DK4", "DK3", "SK2", "END1", "SG7", "far7", "DK5", "SK3", "END3", "DK7",
+    "DK6", "SK0", "END0", "SK5", "END5", "SK4", "END4", "END2", "SK6", "END6", "SK7", "END7",
 )
 BY_ROWS = (V, U, G, E)
 VMEM_BYTES = 67043328
@@ -148,11 +148,17 @@
 
 
 def aligned(index, size):
-    return pl.multiple_of(index * size, size)
-
-
-def layer_kernel(
+    return index * size if isinstance(index, int) else pl.multiple_of(index * size, size)
+
+
+def unit_shares(total):
+    outer = (3 * total // 8) // 256 * 256
+    return outer, total - outer
+
+
+def run_layer(
     fs_size,
+    inner,
     tokens,
     norm_gain,
     ffn_gain,
@@ -194,7 +200,6 @@
     from_side,
     stream,
     pre_gate,
-    hidden,
     total,
     given_down,
     near_down,
@@ -220,6 +225,7 @@
     far_send,
     far_recv,
     out_sem,
+    cross_send,
 ):
     pairs = fs_size // 2
     plane = fs_size // 4
@@ -227,7 +233,7 @@
     level, cell = index // plane, index % plane
     side, column = cell % 2, cell // 2
     low, half = level % 2, level // 2
-    slot = (low + half) % 2
+    slot = int(inner)
     facing = 3 - level
     levels = (level, level + 1 - 2 * low, facing, facing + 1 - 2 * (facing % 2))
     beside, beyond = cell + 1 - 2 * side, cell + 2 - 4 * column
@@ -238,14 +244,21 @@
     mirror = (facing * plane + cell, core)
     across = (level * plane + beside, core)
     over = (level * plane + beyond, core)
-
+    crossed = (levels[3] * plane + cell, core)
+
+    barrier = pltpu.get_barrier_semaphore()
+    for device in (across, over, mate, mirror, crossed, partner):
+        pl.semaphore_signal(barrier, inc=1, device_id=device, device_id_type=MESH)
     own_rows, own_width = tokens.shape
     row_count, full = rows_in.shape
     tile = SEQ_LEN
     tiles = row_count // tile
     half_tiles = tiles // 2
     quarter = whole_v.shape[1]
-    units = whole_gate.shape[1]
+    shares = unit_shares(ffn_gate.shape[1])
+    starts = (0, shares[0])
+    units = shares[slot]
+    relieved = (G, E, W) if inner else ()
     groups = quarter // GROUP_DIM
     spread_width = 2 * 2 * quarter
     block_width = whole_out.shape[2]
@@ -256,20 +269,27 @@
 
     def shard(which, part):
         source = sources[which]
+        if which in (G, E):
+            return source.at[:, pl.ds(starts[part], shares[part])]
+        if which == W:
+            return source.at[pl.ds(starts[part], shares[part]), :]
         if which in BY_ROWS:
             width = source.shape[1] // 2
-            return source.at[:, pl.ds(aligned(part, width), width)]
+            return source.at[:, pl.ds(part * width, width)]
         height = source.shape[0] // 2
-        return source.at[pl.ds(aligned(part, height), height), :]
-
-    def piece(which, at_level, at_cell):
+        return source.at[pl.ds(part * height, height), :]
+
+    def piece(which, at_level, at_cell, part=slot):
         whole = wholes[which]
         if which in BY_ROWS:
+            width = shares[part] if which in (G, E) else whole.shape[1]
             depth_rows = sources[which].shape[0]
-            return whole.at[pl.ds(aligned(at_level * plane + at_cell, depth_rows), depth_rows), :]
+            place = aligned(at_level * plane + at_cell, depth_rows)
+            return whole.at[pl.ds(place, depth_rows), pl.ds(0, width)]
+        height = shares[part] if which == W else whole.shape[1]
         width = sources[which].shape[1]
         block = (at_level // 2) * plane + at_cell
-        return whole.at[block, :, pl.ds(aligned(at_level % 2, width), width)]
+        return whole.at[block, pl.ds(0, height), pl.ds(aligned(at_level % 2, width), width)]
 
     def remote(source, target, send, recv, device):
         return pltpu.make_async_remote_copy(
@@ -289,7 +309,7 @@
     def pool_copy(which):
         return remote(
             shard(which, 1 - slot),
-            piece(which, level, cell),
+            piece(which, level, cell, 1 - slot),
             pool_send.at[which],
             pool_recv.at[which],
             mate,
@@ -304,18 +324,24 @@
         return remote(here, here, flow_send.at[place], flow_recv.at[place], device)
 
     def send_on(which, way, step):
+        device = (across, over)[way]
         if step < 4:
             here = piece(which, levels[step], cell)
+        elif step == 5 and which in relieved:
+            here, device = piece(which, levels[way], diagonal), mirror
         else:
             here = piece(which, levels[2 * (step - 4) + way], (beyond, beside)[way])
-        return moved(which, here, way * 6 + step, (across, over)[way])
+        return moved(which, here, way * 6 + step, device)
 
     def come_in(which, way, step):
+        device = (across, over)[way]
         if step < 4:
             here = piece(which, levels[step], (beside, beyond)[way])
         else:
             here = piece(which, levels[2 * (step - 4) + way], diagonal)
-        moved(which, here, way * 6 + step, (across, over)[way]).wait_recv()
+        if step == 5 and which in relieved:
+            device = mirror
+        moved(which, here, way * 6 + step, device).wait_recv()
 
     def reflect(which, part):
         return moved(which, piece(which, levels[part], cell), 12 + part, mirror)
@@ -338,9 +364,6 @@
     def rows_of(place, height=tile):
         return pl.ds(aligned(place, height), height)
 
-    barrier = pltpu.get_barrier_semaphore()
-    for device in (across, over, mate, mirror, partner):
-        pl.semaphore_signal(barrier, inc=1, device_id=device, device_id_type=MESH)
     for which in (V, U, O):
         own_copy(which).start()
     tokens_in = pltpu.make_async_copy(tokens, token_region(slot, core), local_sem.at[6])
@@ -350,7 +373,7 @@
     for row, vector in enumerate((norm_gain, ffn_gain, layer_gain, layer_shift)):
         values = vector[...].astype(jnp.float32).reshape(1, own_width)
         gains[row : row + 1, pl.ds(aligned(core, own_width), own_width)] = values
-    pl.semaphore_wait(barrier, 5)
+    pl.semaphore_wait(pltpu.get_barrier_semaphore(), 6)
 
     own_tokens = token_region(slot, core)
     def arrive_pool(which):
@@ -399,12 +422,29 @@
         elif step < 4:
             mirror_here(which, step - 2)
         else:
-            flow_here(which, 1 - way, 2 * (step - 4) + way)
+            if step == 5 and which in relieved:
+                flow_here(which, way, 4)
+            else:
+                flow_here(which, 1 - way, 2 * (step - 4) + way)
         send_on(which, way, step).start()
 
+    def cross_copy(which):
+        return remote(
+            shard(which, 1 - slot),
+            piece(which, level, cell, 1 - slot),
+            cross_send.at[which],
+            flow_recv.at[which * 14 + 13],
+            crossed,
+        )
+
     def send_mirror(which, part):
-        part_here(which, part)
-        reflect(which, part).start()
+        if part == 0 or inner:
+            part_here(which, part)
+            reflect(which, part).start()
+
+    def send_cross(which):
+        if inner:
+            cross_copy(which).start()
 
     tokens_in.wait()
     token_copy(1, own_tokens, partner).start()
@@ -422,7 +462,7 @@
             masked[group] = jnp.where(visible, weight, 0.0).astype(jnp.bfloat16)
             lower = bias_rows[group : group + 1]
             upper = bias_rows[group + groups : group + groups + 1]
-            row = jnp.where(slot == 0, lower, upper)
+            row = upper if inner else lower
             bias_cols[group] = jnp.broadcast_to(row, (LANES, BLOCK)).T
 
     first, second = slot * half_tiles, (1 - slot) * half_tiles
@@ -452,7 +492,7 @@
 
         lax.fori_loop(0, tile // step_rows, one, 0)
 
-    def product(target, rows, weights, width, finish):
+    def product(target, rows, weights, width, count, finish):
         def one(part, carry):
             columns = pl.ds(aligned(part, width), width)
             value = jnp.dot(
@@ -461,13 +501,13 @@
             target[rows, columns] = finish(value)
             return carry
 
-        lax.fori_loop(0, weights.shape[1] // width, one, 0)
+        lax.fori_loop(0, count, one, 0)
 
     lane = lax.broadcasted_iota(jnp.int32, (64, LANES), 1)
 
     def act_tile(place, weights, target, with_stats):
         rows = rows_of(place)
-        product(target, rows, weights, 256, lambda value: value)
+        product(target, rows, weights, 256, quarter // 256, lambda value: value)
 
         def one(part, carry):
             some = pl.ds(aligned(place * (tile // 64) + part, 64), 64)
@@ -593,7 +633,7 @@
     def gate_tile(place):
         half_copy(place, other_columns).wait_recv()
         rms_tile(stream, place, 1)
-        product(pre_gate, rows_of(place), whole_gate, 256, to_bfloat)
+        product(pre_gate, rows_of(place), whole_gate, 256, units // 256, to_bfloat)
 
     shifted = lax.broadcasted_iota(jnp.int32, (tile, 256), 0)
 
@@ -607,7 +647,7 @@
 
         def one(part, carry):
             columns = pl.ds(aligned(part, 256), 256)
-            own = pl.ds(aligned(slot * (units // 256) + part, 256), 256)
+            own = pl.ds(aligned(starts[slot] // 256 + part, 256), 256)
             value = jnp.dot(
                 normed[rows, :], whole_value[:, columns], preferred_element_type=jnp.float32
             )
@@ -615,7 +655,7 @@
             gate = pre_gate[rows, columns].astype(jnp.float32)
             conv_g = taps(gate, conv_gate[:, own].astype(jnp.float32))
             conv_v = taps(value, conv_value[:, own].astype(jnp.float32))
-            hidden[rows, columns] = (jax.nn.silu(conv_g) * conv_v).astype(jnp.bfloat16)
+            pre_gate[rows, columns] = (jax.nn.silu(conv_g) * conv_v).astype(jnp.bfloat16)
             return carry
 
         lax.fori_loop(0, units // 256, one, 0)
@@ -650,7 +690,11 @@
 
         def one(part, carry):
             rows = rows_of(which_side * half_tiles + part)
-            value = jnp.dot(hidden[rows, :], whole_down[block], preferred_element_type=jnp.float32)
+            value = jnp.dot(
+                pre_gate[rows, pl.ds(0, units)],
+                whole_down[block, pl.ds(0, units), :],
+                preferred_element_type=jnp.float32,
+            )
             partial[rows, columns] = value.astype(jnp.bfloat16)
             return carry
 
@@ -801,6 +845,8 @@
             block_steps[name[:-1]](int(name[-1]))
         elif name[:4] == "pool":
             pool_copy(NAMES.index(name[4])).start()
+        elif name[:3] == "crs":
+            send_cross(NAMES.index(name[3]))
         elif name[:3] == "mir":
             send_mirror(NAMES.index(name[3]), int(name[4]))
         else:
@@ -815,8 +861,10 @@
         for step in range(6):
             for way in range(2):
                 send_on(which, way, step).wait_send()
-        for part in range(2):
+        for part in range(2 if inner else 1):
             reflect(which, part).wait_send()
+        if inner:
+            cross_copy(which).wait_send()
         pool_copy(which).wait_send()
     for place in range(tiles):
         half_copy(place, own_columns).wait_send()
@@ -839,6 +887,19 @@
     token_copy(3, gain_region(core), partner).wait_send()
     near_stats.wait_send()
     far_stats.wait_send()
+
+
+def layer_kernel(fs_size, *refs):
+    level = lax.axis_index("fs") // (fs_size // 4)
+    middle = (level + level // 2) % 2
+
+    @pl.when(middle == 0)
+    def _():
+        run_layer(fs_size, False, *refs)
+
+    @pl.when(middle == 1)
+    def _():
+        run_layer(fs_size, True, *refs)
 
 
 def on_ring(
@@ -862,7 +923,7 @@
     own_rows, own_width = tokens.shape
     row_count, full = 2 * own_rows, 2 * own_width
     pairs = fs_size // 2
-    quarter, units = proj_u.shape[1] // 2, ffn_gate.shape[1] // 2
+    quarter, units = proj_u.shape[1] // 2, max(unit_shares(ffn_gate.shape[1]))
     groups = quarter // GROUP_DIM
     tiles = row_count // SEQ_LEN
     bf16, f32 = jnp.bfloat16, jnp.float32
@@ -894,7 +955,6 @@
         pltpu.VMEM((row_count, own_width), bf16),
         pltpu.VMEM((row_count, full), bf16),
         pltpu.VMEM((row_count, units), bf16),
-        pltpu.VMEM((row_count, units), bf16),
         pltpu.VMEM((own_rows, own_width), f32),
         pltpu.VMEM((own_rows, own_width), bf16),
         pltpu.VMEM((row_count, own_width), bf16),
@@ -920,6 +980,7 @@
         dma((pairs,)),
         dma((pairs,)),
         dma((2 * pairs,)),
+        dma((6,)),
     ]
     return pl.pallas_call(
         functools.partial(layer_kernel, fs_size),

time: 186 us -> 181 us (0.973)
  Pallas kernels: 183 us -> 179 us
    pallas_call x1, Pallas kernels: 183 us -> 179 us  [on_ring(): pl.pallas_call(functools.partial(layer_kernel, fs_size), out_shape=jax.Sh...]
where the time goes in v4:
time: 181 us
  Pallas kernels  179 us (99%)
  local copies, waits for them, and re-layouts  2.26 us (1%)
    pallas_call x1, Pallas kernels, on_ring(): pl.pallas_call(functools.partial(layer_kernel, fs_size), out_shape=jax.Sh...  179 us

profile of v4, /device:TPU:1, one launch (start us, length us, event | category | flops | bytes accessed | tf_op | source)
XLA Modules:
  0.0 181.3 jit_solution(17259058167107418882)
XLA Ops:
  0.0 179.0 %layer.1 = bf16[512,1024]{1,0:T(8,128)(2,1)} custom-call(bf16[512,1024]{1,0:T(8,128)(2,1)} %refs_0_.1, bf16[1024]{0:T(1024)(128)(2,1)} %refs_1_.1, bf16[1024]{0:T(1024)(128)(2,1)} %refs_2_.1, bf16[1024]{0:T(1024)(128)(2,1)} %refs_3_.1, bf16[1024]{0:T(1024)(128)(2,1)} %refs_4_.1, bf16[8,128,128]{2,1,0:T(8,128)(2,1)} %refs_5_.1, bf16[8,128]{1,0:T(8,128)(2,1)} %refs_6_.1, ...), custom_call_target="tpu_custom_call" | custom-call | tf_op jit(solution)/shard_map/layer/pallas_call | solution.py:985
  179.0 2.3 %copy.17 = bf16[512,1024]{1,0:T(8,128)(2,1)} copy(bf16[512,1024]{1,0:T(8,128)(2,1)} %layer.1) | data formatting | bytes 2097152

commit v5 on v4

--- a/solution.py
+++ b/solution.py
@@ -123,21 +123,22 @@
 V, U, O, G, E, W = range(6)
 NAMES = ("V", "U", "O", "G", "E", "W")
 ORDER = (
-    "yV0", "xG0", "xO0", "yE0", "yG0", "yW0", "poolU", "mirU0", "mirU1", "xU1", "poolV", "xE4",
-    "mirV1", "xV0", "mirV0", "crsV", "poolG", "xV1", "crsU", "crsO", "yU2", "halftok", "poolO",
-    "mirO0", "xU2", "yU0", "yO0", "yV3", "yU4", "xV3", "prep", "Nk0", "crsG", "yV1", "mirO1", "xV4",
-    "xV2", "yU1", "mirE0", "xO4", "xU5", "Nk1", "yV5", "yU3", "yV2", "xU3", "xG1", "poolE", "mirE1",
-    "tok", "poolW", "xU0", "yO1", "yG4", "xV5", "xO3", "mirG0", "xU4", "xO1", "yV4", "yO2", "mirG1",
-    "xG4", "yU5", "xE1", "yG1", "fwd", "Vk1", "xO2", "yO3", "Ng1", "crsE", "Ug1", "yO5", "xE2",
-    "Uk0", "Uk1", "Vg1", "Vk0", "xO5", "Ng0", "yO4", "Vg0", "statA", "statB", "statC", "xG2", "yE4",
-    "Mk0", "yG2", "crsW", "yE1", "xG3", "mirW0", "Ug0", "Mg0", "Mk1", "Ok1", "Ck1", "sidek1", "xE0",
-    "Og0", "yG3", "Cg0", "sideg0", "yE3", "yG5", "Mg1", "Og1", "yE2", "xG5", "xW1", "Cg1", "Ok0",
-    "xE3", "yE5", "Ck0", "Sg1", "sidek0", "yW1", "xW0", "xE5", "Sk0", "Gk0", "yW4", "yW2", "mirW1",
-    "Gg1", "xW4", "sideg1", "Sg0", "xW2", "Gg0", "Eg0", "Eg1", "DG2", "DG1", "DG0", "SG0", "SG2",
-    "far0", "Sk1", "xW3", "DG3", "SG1", "far1", "xW5", "DG4", "far2", "yW3", "Gk1", "yW5", "SG4",
-    "far4", "SG3", "far3", "Ek0", "Ek1", "DK2", "DK1", "DG6", "DG5", "SG6", "far6", "DK0", "SK1",
-    "DG7", "SG5", "far5", "DK4", "DK3", "SK2", "END1", "SG7", "far7", "DK5", "SK3", "END3", "DK7",
-    "DK6", "SK0", "END0", "SK5", "END5", "SK4", "END4", "END2", "SK6", "END6", "SK7", "END7",
+    "yV0", "yU0", "yO0", "yG0", "poolO", "mirU0", "xG0", "xU0", "yO1", "mirO1", "xO1", "poolU",
+    "crsO", "mirU1", "xE0", "poolV", "mirV0", "xU4", "xV4", "xU1", "mirV1", "yW0", "yE0", "poolG",
+    "mirO0", "crsV", "crsU", "xO3", "poolE", "crsE", "crsG", "yV2", "xV1", "yO2", "yV3", "xV3",
+    "yO5", "xU3", "yG1", "mirG0", "prep", "xO4", "xG1", "mirE1", "yV4", "xO0", "yU3", "yV5",
+    "halftok", "yU1", "Nk0", "yU2", "Nk1", "xV2", "yV1", "xE1", "yO3", "xO5", "tok", "xV5", "xV0",
+    "poolW", "yE4", "mirG1", "xG4", "yO4", "yU5", "yU4", "mirW0", "xU2", "fwd", "Vk0", "Ng1", "xO2",
+    "xU5", "yG2", "Vg1", "Ng0", "Vg0", "Vk1", "statA", "xW1", "statB", "yG4", "statC", "xE4", "xG2",
+    "Ug1", "yG3", "crsW", "mirE0", "Mg1", "Og1", "Cg1", "xG5", "sideg1", "Uk1", "Mk1", "Ok1", "Ck1",
+    "Ug0", "Mg0", "Og0", "sidek1", "xG3", "Uk0", "yE2", "yE1", "yG5", "xE3", "xE2", "xE5", "Mk0",
+    "Ok0", "Ck0", "sidek0", "yE5", "Cg0", "sideg0", "yE3", "yW4", "Sk1", "Gk1", "mirW1", "xW4",
+    "yW1", "Sg1", "Gg1", "Sg0", "Gg0", "xW0", "yW2", "Eg1", "Eg0", "DG0", "xW3", "xW5", "Sk0",
+    "DG4", "SG0", "far0", "DG3", "yW3", "SG4", "far4", "Gk0", "yW5", "DG2", "DG1", "SG3", "far3",
+    "Ek0", "xW2", "SG1", "far1", "Ek1", "DK1", "DK3", "SG2", "far2", "DG7", "DK4", "SK1", "END1",
+    "SG7", "far7", "DK7", "DG6", "SK3", "SK7", "DK2", "SG6", "far6", "DG5", "DK0", "SK2", "END3",
+    "SG5", "far5", "END2", "DK5", "SK4", "END4", "SK0", "DK6", "END7", "SK6", "END6", "SK5", "END0",
+    "END5",
 )
 BY_ROWS = (V, U, G, E)
 VMEM_BYTES = 67043328

time: 181 us -> 179 us (0.989)
  Pallas kernels: 179 us -> 177 us
    pallas_call x1, Pallas kernels: 179 us -> 177 us  [on_ring(): pl.pallas_call(functools.partial(layer_kernel, fs_size), out_shape=jax.Sh...]
where the time goes in v5:
time: 179 us
  Pallas kernels  177 us (99%)
  local copies, waits for them, and re-layouts  2.26 us (1%)
    pallas_call x1, Pallas kernels, on_ring(): pl.pallas_call(functools.partial(layer_kernel, fs_size), out_shape=jax.Sh...  177 us

profile of v5, /device:TPU:1, one launch (start us, length us, event | category | flops | bytes accessed | tf_op | source)
XLA Modules:
  0.0 179.1 jit_solution(18324559598037868671)
XLA Ops:
  0.0 176.8 %layer.1 = bf16[512,1024]{1,0:T(8,128)(2,1)} custom-call(bf16[512,1024]{1,0:T(8,128)(2,1)} %refs_0_.1, bf16[1024]{0:T(1024)(128)(2,1)} %refs_1_.1, bf16[1024]{0:T(1024)(128)(2,1)} %refs_2_.1, bf16[1024]{0:T(1024)(128)(2,1)} %refs_3_.1, bf16[1024]{0:T(1024)(128)(2,1)} %refs_4_.1, bf16[8,128,128]{2,1,0:T(8,128)(2,1)} %refs_5_.1, bf16[8,128]{1,0:T(8,128)(2,1)} %refs_6_.1, ...), custom_call_target="tpu_custom_call" | custom-call | tf_op jit(solution)/shard_map/layer/pallas_call | solution.py:986
  176.8 2.3 %copy.17 = bf16[512,1024]{1,0:T(8,128)(2,1)} copy(bf16[512,1024]{1,0:T(8,128)(2,1)} %layer.1) | data formatting | bytes 2097152
